TPU v7x, 1024 devices: a whole 4x8x16 slice. The times are simulated.
1024 devices in a mesh: fs: 16 (over z), rep: 8 (over y), tp: 8 (over x, core).
Axes of the slice: x: 4, y: 8, z: 16, core: 2. Of those that a mesh axis runs over, the one named last changes fastest.
Arguments:
- saved_hidden: bfloat16 [114688, 2048], P(('fs', 'rep')), may hold values from -12 to 12
- grad_value: bfloat16 [114688, 1024], P(('fs', 'rep'), 'tp'), may hold values from -12 to 12
- saved_mixed: bfloat16 [114688, 1024], P(('fs', 'rep'), 'tp'), may hold values from -12 to 12
- grad_output: bfloat16 [114688, 2048], P(('fs', 'rep')), may hold values from -12 to 12
- basis_value: bfloat16 [2048, 128], replicated, may hold values from -0.5 to 0.5
- basis_output: bfloat16 [2048, 128], replicated, may hold values from -0.5 to 0.5
- weight_value: float32 [2048, 1024], P('fs', 'tp'), may hold values from -0.125 to 0.125
- weight_output: float32 [1024, 2048], P('tp', 'fs'), may hold values from -0.1875 to 0.1875
- first_value: float32 [128, 1024], P('fs', 'tp'), may hold values from -4 to 4
- second_value: float32 [128, 1024], P('fs', 'tp'), may hold values from 0.05 to 0.5
- first_output: float32 [128, 1024], P('fs', 'tp'), may hold values from -4 to 4
- second_output: float32 [128, 1024], P('fs', 'tp'), may hold values from 0.05 to 0.5
Outputs:
- step_value: float32 [2048, 1024], P('fs', 'tp')
- step_output: float32 [1024, 2048], P('tp', 'fs')
- new_weight_value: float32 [2048, 1024], P('fs', 'tp')
- new_weight_output: float32 [1024, 2048], P('tp', 'fs')
- copy_value: bfloat16 [2048, 1024], P(None, 'tp')
- copy_output: bfloat16 [1024, 2048], P('tp')
- new_first_value: float32 [128, 1024], P('fs', 'tp')
- new_second_value: float32 [128, 1024], P('fs', 'tp')
- new_first_output: float32 [128, 1024], P('fs', 'tp')
- new_second_output: float32 [128, 1024], P('fs', 'tp')
All inputs are finite; a program needn't handle non-finite values.
Results may differ from a plain program's by a relative error of at most 0.0045.
Values may be sent and summed in bfloat16 or wider, within the bound.
No kernel may reach another device: no remote copies, remote signals or barrier semaphores. Data moves between devices by JAX's collectives and lax.ppermute only.
A program may use at most 32 MiB of HBM per device.

v0:
```python
import jax
import jax.numpy as jnp
from jax import lax
from jax.sharding import PartitionSpec as P

AW = 1024
RANK = 128


first_decay = 0.8
second_decay = 0.9
learning_rate = 0.02
norm_epsilon = 1e-06
contract_leading = (((0,), (0,)), ((), ()))


def side_by_side(arrays, axis, dim, along):
    widths = [a.shape[along] for a in arrays]
    both = jnp.concatenate(arrays, axis=along)
    filled = lax.all_gather(both, axis, axis=dim, tiled=True)
    return tuple(jnp.split(filled, [sum(widths[:k]) for k in range(1, len(widths))], axis=along))


def one_axis_at_a_time(shard, axes):
    for axis in axes:
        shard = lax.psum(shard, axis)
    return shard


def rows_first(arrays, axis, dims):
    turned = [jnp.moveaxis(a, dim, 0) for a, dim in zip(arrays, dims)]
    both = jnp.concatenate([t.reshape(len(t), -1) for t in turned], axis=1)
    filled, at, done = (lax.all_gather(both, axis, axis=0, tiled=True), 0, [])
    for t, dim in zip(turned, dims):
        share = filled[:, at : at + t[0].size].reshape(-1, *t.shape[1:])
        done.append(jnp.moveaxis(share, 0, dim))
        at += t[0].size
    return tuple(done)


def moments(projected, first_old, second_old, clip_factor):
    scaled = clip_factor * projected
    first_new = first_decay * first_old + (1.0 - first_decay) * scaled
    second_new = second_decay * second_old + (1.0 - second_decay) * scaled * scaled
    return (first_new, second_new, first_new / jnp.sqrt(second_new))


def split_product(reduced, other):
    upper = reduced.astype(jnp.bfloat16)
    lower = (reduced - upper.astype(jnp.float32)).astype(jnp.bfloat16)
    rank_count = reduced.shape[1]
    stacked = jnp.concatenate([upper, lower], axis=1)
    both = lax.dot_general(stacked, other, contract_leading, preferred_element_type=jnp.float32)
    return both[:rank_count] + both[rank_count:]


def local(
    saved_hidden,
    grad_value,
    saved_mixed,
    grad_output,
    basis_value,
    basis_output,
    weight_value,
    weight_output,
    first_value,
    second_value,
    first_output,
    second_output,
):
    row_count = weight_value.shape[0]
    moment_count = first_value.shape[0]
    fs_index = lax.axis_index("fs")
    row_first = fs_index * row_count
    moment_first = fs_index * moment_count
    value_basis_rows = lax.dynamic_slice_in_dim(basis_value, row_first, row_count, 0).astype(
        jnp.float32
    )
    output_basis_rows = lax.dynamic_slice_in_dim(basis_output, row_first, row_count, 0).astype(
        jnp.float32
    )
    whole_moments = side_by_side(
        (first_value, second_value, first_output, second_output), "fs", 0, 1
    )
    reduced_hidden = jnp.dot(saved_hidden, basis_value, preferred_element_type=jnp.float32)
    reduced_output = jnp.dot(grad_output, basis_output, preferred_element_type=jnp.float32)
    part_value = split_product(reduced_hidden, grad_value)
    part_output = split_product(reduced_output, saved_mixed)
    projected_value, projected_output = (
        one_axis_at_a_time(part_value, ("fs", "rep")),
        one_axis_at_a_time(part_output, ("fs", "rep")),
    )
    local_squares = jnp.sum(projected_value * projected_value) + jnp.sum(
        projected_output * projected_output
    )
    total_squares = lax.psum(local_squares, "tp")
    mean_square = total_squares / (2 * RANK * AW)
    clip_factor = jnp.minimum(1.0, 1.0 / jnp.sqrt(mean_square + norm_epsilon))
    whole_first_value, whole_second_value, whole_first_output, whole_second_output = whole_moments
    first_all_value, second_all_value, direction_value = moments(
        projected_value, whole_first_value, whole_second_value, clip_factor
    )
    first_all_output, second_all_output, direction_output = moments(
        projected_output, whole_first_output, whole_second_output, clip_factor
    )
    new_first_value = lax.dynamic_slice_in_dim(first_all_value, moment_first, moment_count, 0)
    new_second_value = lax.dynamic_slice_in_dim(second_all_value, moment_first, moment_count, 0)
    new_first_output = lax.dynamic_slice_in_dim(first_all_output, moment_first, moment_count, 0)
    new_second_output = lax.dynamic_slice_in_dim(second_all_output, moment_first, moment_count, 0)
    step_value = jnp.dot(value_basis_rows, direction_value, precision=lax.Precision.HIGHEST)
    step_output = jnp.dot(output_basis_rows, direction_output, precision=lax.Precision.HIGHEST).T
    new_weight_value = weight_value - learning_rate * step_value
    new_weight_output = weight_output - learning_rate * step_output
    copy_value, copy_output = rows_first(
        (new_weight_value.astype(jnp.bfloat16), new_weight_output.astype(jnp.bfloat16)),
        "fs",
        (0, 1),
    )
    return (
        step_value,
        step_output,
        new_weight_value,
        new_weight_output,
        copy_value,
        copy_output,
        new_first_value,
        new_second_value,
        new_first_output,
        new_second_output,
    )


def solution(mesh):
    return jax.shard_map(
        local,
        mesh=mesh,
        in_specs=(
            P(("fs", "rep"), None),
            P(("fs", "rep"), "tp"),
            P(("fs", "rep"), "tp"),
            P(("fs", "rep"), None),
            P(),
            P(),
            P("fs", "tp"),
            P("tp", "fs"),
            P("fs", "tp"),
            P("fs", "tp"),
            P("fs", "tp"),
            P("fs", "tp"),
        ),
        out_specs=(
            P("fs", "tp"),
            P("tp", "fs"),
            P("fs", "tp"),
            P("tp", "fs"),
            P(None, "tp"),
            P("tp", None),
            P("fs", "tp"),
            P("fs", "tp"),
            P("fs", "tp"),
            P("fs", "tp"),
        ),
        check_vma=False,
    )
```

profile of v0, /device:TPU:6, one launch (start us, length us, event | category | flops | bytes accessed | tf_op | source)
XLA Modules:
  0.0 356.1 jit_solution(6655842066924168234)
XLA Ops:
  7.2 0.0 copy-start
  7.2 0.0 copy-start.2
  7.2 0.0 copy-start.10
  7.2 0.0 all-reduce.5.cloned.1.call-start
  7.3 1.0 copy-done
  8.2 3.4 subtract_convert_fusion.1
  11.6 0.0 copy-done.2
  11.6 0.0 copy-done.1
  11.7 0.0 copy-start.11
  11.7 0.0 copy-start.6
  11.7 0.0 copy-start.7
  11.7 0.0 copy-start.8
  11.7 0.0 copy-start.9
  11.7 0.0 copy-start.5
  11.7 0.0 copy-start.4
  11.7 1.2 subtract_convert_fusion
  13.0 0.0 copy-done.10
  13.0 0.3 fusion
  13.3 0.0 copy-done.11
  13.3 0.3 fusion.4
  13.6 0.7 slice_add_fusion
  14.2 0.0 all-reduce.5.cloned.1.call-update
  14.3 0.0 all-reduce.7.cloned.1.call-start
  14.3 151.5 %all-reduce.5.cloned.1.call-done = (f32[128,128]{1,0:T(8,128)}, f32[128,128]{1,0:T(8,128)}) async-done(((f32[128,128]{1,0:T(8,128)}, f32[128,128]{1,0:T(8,128)}), (f32[128,128]{1,0:T(8,128)}, f32[128,128]{1,0:T(8,128)})) %all-reduce.5.cloned.1.call-update) | async-done | bytes 131088 | tf_op jit(solution)/shard_map/psum | solution.py:26
  165.8 0.0 all-reduce.7.cloned.1.call-update
  165.8 0.0 all-gather.2.cloned.1.call-start
  165.9 0.1 copy.23
  166.0 29.6 %all_gather.6 = f32[128,512]{1,0:T(8,128)S(1)} all-gather(f32[8,512]{1,0:T(8,128)S(1)} %pad_maximum_fusion.1), channel_id=1, replica_groups=mesh['fs'=16,'rep'=8,'tp'=8] {'fs'}, dimensions={0}, use_global_device_ids=true | all-gather | bytes 278528 | tf_op jit(solution)/shard_map/all_gather | solution.py:20
  195.6 57.5 %all-reduce.7.cloned.1.call-done = (f32[128,128]{1,0:T(8,128)}, f32[128,128]{1,0:T(8,128)}) async-done(((f32[128,128]{1,0:T(8,128)}, f32[128,128]{1,0:T(8,128)}), (f32[128,128]{1,0:T(8,128)}, f32[128,128]{1,0:T(8,128)})) %all-reduce.7.cloned.1.call-update) | async-done | bytes 131088 | tf_op jit(solution)/shard_map/psum | solution.py:26
  253.2 1.5 multiply_reduce_fusion
  254.6 1.5 multiply_reduce_fusion.1
  257.4 10.5 %psum.39 = f32[]{:T(128)} all-reduce(f32[]{:T(128)S(6)} %add.47), channel_id=1, replica_groups=mesh['fs'=16,'rep'=8,'tp'=8] {'tp'}, use_global_device_ids=true, to_apply=%region_6.0 | all-reduce | flops 1 | bytes 8 | tf_op jit(solution)/shard_map/psum | solution.py:96
  268.6 0.9 fusion.9
  269.5 0.3 fusion.12
  269.8 0.0 copy-start.3
  269.8 0.6 convert_bitcast_fusion
  270.4 0.3 fusion.24
  270.7 0.6 pad_maximum_fusion
  271.3 0.0 all-gather.2.cloned.1.call-update
  271.4 0.7 copy.25
  272.1 0.7 copy.24
  272.8 0.6 constant_dynamic-slice_fusion
  273.4 0.6 constant_dynamic-slice_fusion.1
  274.0 0.6 constant_dynamic-slice_fusion.3
  274.6 0.6 constant_dynamic-slice_fusion.2
  275.2 71.3 %all-gather.2.cloned.1.call-done = bf16[2048,256]{0,1:T(8,128)(2,1)} async-done(((bf16[128,256]{0,1:T(8,128)(2,1)}), bf16[2048,256]{0,1:T(8,128)(2,1)}) %all-gather.2.cloned.1.call-update) | async-done | bytes 1048592 | tf_op jit(solution)/shard_map/all_gather | solution.py:33
  346.5 2.1 slice_bitcast_fusion
  348.6 1.0 copy.26
  (9 shorter events, 0.0 us)
Async XLA Ops:
  7.2 1.0 copy-start
  7.2 4.4 %copy-start.2 = (bf16[2048,128]{1,0:T(8,128)(2,1)S(1)}, bf16[2048,128]{1,0:T(8,128)(2,1)}, u32[]{:S(2)}) copy-start(bf16[2048,128]{1,0:T(8,128)(2,1)} %param.17) | copy-start | bytes 1572868
  7.2 5.8 %copy-start.10 = (bf16[896,128]{1,0:T(8,128)(2,1)S(1)}, bf16[896,128]{1,0:T(8,128)(2,1)}, u32[]{:S(2)}) copy-start(bf16[896,128]{1,0:T(8,128)(2,1)} %param.13) | copy-start | bytes 688132
  7.2 158.6 %all-reduce.5.cloned.1.call-start = ((), (), s32[]{:S(2)}) async-start(), calls=%async_computation.1 | async-start | bytes 262144 | tf_op jit(solution)/shard_map/psum | solution.py:26
  8.2 3.4 copy-start.1
  11.7 1.6 copy-start.11
  11.7 154.2 %copy-start.6 = (f32[8,128]{1,0:T(8,128)S(1)}, f32[8,128]{1,0:T(8,128)}, u32[]{:S(2)}) copy-start(f32[8,128]{1,0:T(8,128)} %param.23) | copy-start | bytes 12292
  11.7 154.2 %copy-start.7 = (f32[8,128]{1,0:T(8,128)S(1)}, f32[8,128]{1,0:T(8,128)}, u32[]{:S(2)}) copy-start(f32[8,128]{1,0:T(8,128)} %param.22) | copy-start | bytes 12292
  11.7 154.2 %copy-start.8 = (f32[8,128]{1,0:T(8,128)S(1)}, f32[8,128]{1,0:T(8,128)}, u32[]{:S(2)}) copy-start(f32[8,128]{1,0:T(8,128)} %param.21) | copy-start | bytes 12292
  11.7 154.2 %copy-start.9 = (f32[8,128]{1,0:T(8,128)S(1)}, f32[8,128]{1,0:T(8,128)}, u32[]{:S(2)}) copy-start(f32[8,128]{1,0:T(8,128)} %param.20) | copy-start | bytes 12292
  11.7 154.2 %copy-start.5 = (f32[128,128]{1,0:T(8,128)S(1)}, f32[128,128]{1,0:T(8,128)}, u32[]{:S(2)}) copy-start(f32[128,128]{1,0:T(8,128)} %param.18) | copy-start | bytes 196612
  11.7 258.0 %copy-start.4 = (f32[128,128]{1,0:T(8,128)S(1)}, f32[128,128]{1,0:T(8,128)}, u32[]{:S(2)}) copy-start(f32[128,128]{1,0:T(8,128)} %param.19) | copy-start | bytes 196612
  14.3 238.9 %all-reduce.7.cloned.1.call-start = ((), (), s32[]{:S(2)}) async-start(), calls=%async_computation.2 | async-start | bytes 262144 | tf_op jit(solution)/shard_map/psum | solution.py:26
  165.8 180.7 %all-gather.2.cloned.1.call-start = ((), (), s32[]{:S(2)}) async-start(), calls=%async_computation | async-start | bytes 1114112 | tf_op jit(solution)/shard_map/all_gather | solution.py:33
  269.8 79.8 %copy-start.3 = (f32[128,128]{1,0:T(8,128)}, f32[128,128]{1,0:T(8,128)S(1)}, u32[]{:S(2)}) copy-start(f32[128,128]{1,0:T(8,128)S(1)} %fusion.12) | copy-start | bytes 196612
Sparse Core Ops, SparseCore 0:
  14.4 151.3 all-reduce.4
  168.2 84.9 all-reduce.6
  271.5 74.9 all-gather.1
where the time goes:
time: 357 us; the launch traced here: 356 us
  waiting for transfers between devices  280 us (78%)
  blocking collectives  40.1 us (11%)
  between operations  16 us (4%)
  local copies, waits for them, and re-layouts  8.04 us (2%)
  other arithmetic  5.79 us (2%)
  matrix products  5.69 us (2%)
    psum x2, waiting for transfers between devices, one_axis_at_a_time(): shard = lax.psum(shard, axis)  209 us
    all_gather x1, waiting for transfers between devices, rows_first(): filled, at, done = (lax.all_gather(both, axis, axis=0, tiled=True), 0, [])  71.3 us
    all_gather x1, blocking collectives, side_by_side(): filled = lax.all_gather(both, axis, axis=dim, tiled=True)  29.6 us
    psum x1, blocking collectives, local(): total_squares = lax.psum(local_squares, 'tp')  10.5 us
  transfers between devices with their start and end apart: 3, of which 3 were waited for; matrix products, arithmetic and copies ran while one was open for 1% of the time, Pallas kernels for 0%

commit v1 on v0

v1 whole, which is shorter than its diff:
```python
import jax
import jax.numpy as jnp
from jax import lax
from jax.sharding import PartitionSpec as P


AW = 1024
RANK = 128


first_decay = 0.8
second_decay = 0.9
learning_rate = 0.02
norm_epsilon = 1e-06
f32 = jnp.float32
bf16 = jnp.bfloat16
contract_leading = (((0,), (0,)), ((), ()))


def exchange(chunks, axes):
    return lax.all_to_all(chunks, axes, 0, 0, tiled=True)


def split(array):
    upper = array.astype(bf16)
    return upper, (array - upper.astype(f32)).astype(bf16)


def moments(projected, first_old, second_old, clip_factor):
    scaled = clip_factor * projected
    first_new = first_decay * first_old + (1.0 - first_decay) * scaled
    second_new = second_decay * second_old + (1.0 - second_decay) * scaled * scaled
    return (first_new, second_new, first_new / jnp.sqrt(second_new))


def split_product(reduced, other):
    upper, lower = split(reduced)
    stacked = jnp.concatenate([upper, lower], axis=1)
    both = lax.dot_general(stacked, other, contract_leading, preferred_element_type=f32)
    rank_count = reduced.shape[1]
    return both[:rank_count] + both[rank_count:]


def local(
    saved_hidden,
    grad_value,
    saved_mixed,
    grad_output,
    basis_value,
    basis_output,
    weight_value,
    weight_output,
    first_value,
    second_value,
    first_output,
    second_output,
):
    fs, rep, tp = lax.axis_size("fs"), lax.axis_size("rep"), lax.axis_size("tp")
    fs_index = lax.axis_index("fs")
    rep_index = lax.axis_index("rep")
    rows, columns = weight_value.shape
    cut = rows // rep
    ranks = first_value.shape[0]
    width = RANK // (rep * tp)

    old = jnp.stack([first_value, second_value, first_output, second_output])
    old_piece = lax.dynamic_slice_in_dim(old, rep_index, 1, 1).reshape(4, columns)
    old_upper, old_lower = split(old_piece)
    piece = jnp.concatenate(
        [
            lax.dynamic_slice_in_dim(weight_value, rep_index * cut, cut, 0).astype(bf16),
            lax.dynamic_slice_in_dim(weight_output, rep_index * cut, cut, 0).astype(bf16),
            old_upper,
            old_lower,
        ]
    )
    spread = jnp.broadcast_to(piece[None], (fs, *piece.shape))
    pieces = exchange(spread, "fs")
    gathered = lax.all_gather(pieces, "rep")

    reduced_hidden = jnp.dot(saved_hidden, basis_value, preferred_element_type=f32)
    reduced_output = jnp.dot(grad_output, basis_output, preferred_element_type=f32)
    part_value = split_product(reduced_hidden, grad_value)
    part_output = split_product(reduced_output, saved_mixed)

    part = jnp.stack(
        [part_value.reshape(-1, width, columns), part_output.reshape(-1, width, columns)], axis=1
    ).reshape(rep * tp, 2 * width, columns)
    part = exchange(part, ("rep", "tp"))
    part = jnp.sum(part.reshape(rep, tp, 2 * width, columns), axis=0)
    part = jnp.broadcast_to(part.astype(bf16)[None], (fs, *part.shape))
    part = exchange(part.reshape(fs, tp * 2 * width, columns), "fs")
    whole = jnp.sum(part.astype(f32), axis=0).reshape(tp, 2 * width, columns)

    squares = jnp.broadcast_to(jnp.sum(whole * whole), (tp, 1, columns))
    square_upper, square_lower = split(squares)
    back = jnp.concatenate(
        [whole.astype(bf16), square_upper, square_lower, square_lower, square_lower], axis=1
    )[:, :8]
    back = jnp.broadcast_to(back[None], (rep, *back.shape)).reshape(rep * tp, *back.shape[1:])
    back = exchange(back, ("rep", "tp")).astype(f32)
    projected_value = back[:, :width].reshape(RANK, columns)
    projected_output = back[:, width : 2 * width].reshape(RANK, columns)
    total_squares = jnp.sum(back[:, 2 * width, 0] + back[:, 2 * width + 1, 0])
    mean_square = total_squares / (2 * RANK * AW)
    clip_factor = jnp.minimum(1.0, 1.0 / jnp.sqrt(mean_square + norm_epsilon))

    old = gathered[:, :, 2 * cut :].astype(f32)
    old = old[:, :, :4] + old[:, :, 4:]
    old = old.transpose(2, 1, 0, 3).reshape(4, RANK, columns)
    direction_value = moments(projected_value, old[0], old[1], clip_factor)[2]
    direction_output = moments(projected_output, old[2], old[3], clip_factor)[2]
    moment_first = fs_index * ranks
    new_first_value, new_second_value, _ = moments(
        lax.dynamic_slice_in_dim(projected_value, moment_first, ranks, 0),
        first_value,
        second_value,
        clip_factor,
    )
    new_first_output, new_second_output, _ = moments(
        lax.dynamic_slice_in_dim(projected_output, moment_first, ranks, 0),
        first_output,
        second_output,
        clip_factor,
    )

    value_upper, value_lower = split(direction_value)
    output_upper, output_lower = split(direction_output)

    def value_step(basis):
        return jnp.dot(basis, value_upper, preferred_element_type=f32) + jnp.dot(
            basis, value_lower, preferred_element_type=f32
        )

    def output_step(basis):
        across = (((0,), (1,)), ((), ()))
        return lax.dot_general(
            output_upper, basis, across, preferred_element_type=f32
        ) + lax.dot_general(output_lower, basis, across, preferred_element_type=f32)

    value_rows = lax.dynamic_slice_in_dim(basis_value, fs_index * rows, rows, 0)
    output_rows = lax.dynamic_slice_in_dim(basis_output, fs_index * rows, rows, 0)
    step_value = value_step(value_rows)
    step_output = output_step(output_rows)
    new_weight_value = weight_value - learning_rate * step_value
    new_weight_output = weight_output - learning_rate * step_output
    whole_value = gathered[:, :, :cut].transpose(1, 0, 2, 3).reshape(fs * rows, columns)
    whole_output = gathered[:, :, cut : 2 * cut].transpose(0, 2, 1, 3).reshape(rows, fs * columns)
    copy_value = (whole_value.astype(f32) - learning_rate * value_step(basis_value)).astype(bf16)
    copy_output = (whole_output.astype(f32) - learning_rate * output_step(basis_output)).astype(
        bf16
    )
    return (
        step_value,
        step_output,
        new_weight_value,
        new_weight_output,
        copy_value,
        copy_output,
        new_first_value,
        new_second_value,
        new_first_output,
        new_second_output,
    )


def solution(mesh):
    return jax.shard_map(
        local,
        mesh=mesh,
        in_specs=(
            P(("fs", "rep"), None),
            P(("fs", "rep"), "tp"),
            P(("fs", "rep"), "tp"),
            P(("fs", "rep"), None),
            P(),
            P(),
            P("fs", "tp"),
            P("tp", "fs"),
            P("fs", "tp"),
            P("fs", "tp"),
            P("fs", "tp"),
            P("fs", "tp"),
        ),
        out_specs=(
            P("fs", "tp"),
            P("tp", "fs"),
            P("fs", "tp"),
            P("tp", "fs"),
            P(None, "tp"),
            P("tp", None),
            P("fs", "tp"),
            P("fs", "tp"),
            P("fs", "tp"),
            P("fs", "tp"),
        ),
        check_vma=False,
    )
```

time: 357 us -> 132 us (0.37)
  the two profiles are of different devices: /device:TPU:6 before, /device:TPU:1 now
where the time goes in v1:
time: 132 us; the launch traced here: 131 us
  blocking collectives  41.4 us (31%)
  starting transfers between devices  26.8 us (20%)
  waiting for transfers between devices  18.1 us (14%)
  between operations  16.4 us (12%)
  matrix products  12.7 us (10%)
  local copies, waits for them, and re-layouts  11 us (8%)
  other arithmetic  4.59 us (3%)
    all_to_all x2, blocking collectives, exchange(): return lax.all_to_all(chunks, axes, 0, 0, tiled=True)  41.4 us
    all_to_all x2, starting transfers between devices, exchange(): return lax.all_to_all(chunks, axes, 0, 0, tiled=True)  26.7 us
    all_to_all x2, waiting for transfers between devices, exchange(): return lax.all_to_all(chunks, axes, 0, 0, tiled=True)  18.1 us
    convert_element_type x2, local copies, waits for them, and re-layouts, local(): whole_value.astype(f32) - learning_rate * value_step(basis_value)  3.64 us
    dot_general x1, matrix products, local(): jnp.dot(saved_hidden, basis_value, preferred_element_type=f32)  3.4 us
    dot_general x2, matrix products, output_step(): lax.dot_general(output_lower, basis, across, preferred_element_type=f32)  3.39 us
    dot_general x2, matrix products, value_step(): jnp.dot(basis, value_lower, preferred_element_type=f32)  3.14 us
    unnamed x26, local copies, waits for them, and re-layouts  2.78 us
  transfers between devices with their start and end apart: 3, of which 2 were waited for; matrix products, arithmetic and copies ran while one was open for 6% of the time, Pallas kernels for 0%

profile of v1, /device:TPU:1, one launch (start us, length us, event | category | flops | bytes accessed | tf_op | source)
XLA Modules:
  0.0 130.9 jit_solution(2438517642836722383)
XLA Ops:
  7.2 0.0 copy-start
  7.2 0.0 copy-start.10
  7.2 0.8 fusion.43
  8.1 0.7 dynamic-slice_convert_fusion
  8.8 0.7 broadcast_in_dim.10
  9.5 19.4 %all-to-all-start = ((bf16[16,40,128]{2,1,0:T(8,128)(2,1)}), bf16[16,40,128]{2,1,0:T(8,128)(2,1)S(1)}, u32[]{:S(2)}, u32[]{:S(2)}) async-start(bf16[16,40,128]{2,1,0:T(8,128)(2,1)} %broadcast_in_dim.10), calls=%async_computation | async-start | bytes 327680 | tf_op jit(solution)/shard_map/all_to_all | solution.py:21
  28.9 0.0 all-gather.3.cloned.1.call-start
  29.0 0.0 copy-start.2
  29.0 3.4 %subtract_convert_fusion.1 = (bf16[896,128]{0,1:T(8,128)(2,1)S(1)}, bf16[896,128]{0,1:T(8,128)(2,1)S(1)}) fusion(bf16[896,2048]{1,0:T(8,128)(2,1)} %param.12, bf16[2048,128]{1,0:T(8,128)(2,1)S(1)} %copy-done), kind=kOutput, calls=%fused_computation.22 | convolution fusion | flops 470220800 | bytes 4653056 | tf_op jit(solution)/shard_map/dot_general | solution.py:81
  32.4 0.0 copy-start.11
  32.4 0.3 fusion.7
  32.7 0.0 copy-start.6
  32.7 0.0 copy-start.7
  32.7 0.0 copy-start.8
  32.7 0.0 copy-start.9
  32.8 1.2 subtract_convert_fusion
  34.0 0.3 fusion.11
  34.3 6.8 %all-to-all-done = bf16[16,40,128]{2,1,0:T(8,128)(2,1)S(1)} async-done(((bf16[16,40,128]{2,1,0:T(8,128)(2,1)}), bf16[16,40,128]{2,1,0:T(8,128)(2,1)S(1)}, u32[]{:S(2)}, u32[]{:S(2)}) %all-to-all-start) | async-done | bytes 163872 | tf_op jit(solution)/shard_map/all_to_all | solution.py:21
  41.1 0.7 copy-done.3
  41.7 0.0 all-gather.3.cloned.1.call-update
  41.8 0.1 copy.85
  41.9 25.6 %all_to_all.20 = f32[64,4,128]{2,1,0:T(4,128)S(1)} all-to-all(f32[64,4,128]{2,1,0:T(4,128)S(1)} %copy.85), channel_id=1, replica_groups=mesh['fs'=16,'rep'=8,'tp'=8] {'rep','tp'}, dimensions={0} | all-to-all | bytes 262144 | tf_op jit(solution)/shard_map/all_to_all | solution.py:21
  67.6 15.8 %all_to_all.21 = bf16[16,32,128]{2,1,0:T(8,128)(2,1)S(1)} all-to-all(bf16[16,32,128]{2,1,0:T(8,128)(2,1)S(1)} %broadcast_in_dim.11), channel_id=1, replica_groups=mesh['fs'=16,'rep'=8,'tp'=8] {'fs'}, dimensions={0} | all-to-all | bytes 262144 | tf_op jit(solution)/shard_map/all_to_all | solution.py:21
  83.4 0.6 multiply_reduce_fusion
  85.3 0.1 concatenate.15
  85.4 0.7 broadcast_in_dim.27
  86.1 7.3 %all-to-all-start.3 = ((bf16[64,8,128]{2,1,0:T(8,128)(2,1)}), bf16[64,8,128]{2,1,0:T(8,128)(2,1)S(1)}, u32[]{:S(2)}, u32[]{:S(2)}) async-start(bf16[64,8,128]{2,1,0:T(8,128)(2,1)} %bitcast.14), calls=%async_computation.3 | async-start | bytes 262144 | tf_op jit(solution)/shard_map/all_to_all | solution.py:21
  93.4 11.3 %all-to-all-done.3 = bf16[64,8,128]{2,1,0:T(8,128)(2,1)S(1)} async-done(((bf16[64,8,128]{2,1,0:T(8,128)(2,1)}), bf16[64,8,128]{2,1,0:T(8,128)(2,1)S(1)}, u32[]{:S(2)}, u32[]{:S(2)}) %all-to-all-start.3) | async-done | bytes 131104 | tf_op jit(solution)/shard_map/all_to_all | solution.py:21
  104.7 0.7 fusion.28
  106.2 0.6 fusion.35
  106.8 1.0 slice.72
  107.8 0.0 copy-start.4
  107.8 1.5 %convert_bitcast_fusion = (f32[8,16,16,128]{3,1,2,0:T(8,128)S(1)}, f32[16,8,16,128]{3,2,0,1:T(8,128)S(1)}) fusion(bf16[8,16,40,128]{3,2,1,0:T(8,128)(2,1)} %bitcast.65), kind=kLoop, calls=%fused_computation.11 | loop fusion | flops 524288 | bytes 3145728 | tf_op jit(solution)/shard_map/convert_element_type | solution.py:150
  109.3 0.0 copy-start.5
  109.3 0.2 copy_convert_fusion
  109.5 0.1 fusion.21
  109.6 0.3 fusion.46
  109.9 0.2 fusion.30
  110.1 0.1 fusion.33
  110.2 0.3 fusion.49
  110.5 0.8 multiply_subtract_fusion.1
  111.3 0.8 multiply_subtract_fusion
  112.2 1.3 copy.90
  113.5 1.1 copy.88
  114.6 2.5 %copy.89 = f32[2048,128]{0,1:T(8,128)} copy(f32[2048,128]{1,0:T(8,128)} %bitcast.63) | data formatting | bytes 2097152 | tf_op jit(solution)/shard_map/convert_element_type | solution.py:149
  117.1 2.3 %fusion.5 = bf16[2048,128]{0,1:T(8,128)(2,1)} fusion(f32[2048,128]{0,1:T(8,128)} %copy.89, f32[128,2048]{1,0:T(8,128)S(1)} %fusion.49, bf16[2048,128]{1,0:T(8,128)(2,1)S(1)} %copy-done, f32[128,128]{1,0:T(8,128)S(1)} %get-tuple-element.89), kind=kOutput, calls=%fused_computation.7 | convolution fusion | flops 68222976 | bytes 3211264 | tf_op jit(solution)/shard_map/dot_general | solution.py:131
  119.5 2.0 %copy.91 = bf16[2048,128]{1,0:T(8,128)(2,1)} copy(bf16[2048,128]{0,1:T(8,128)(2,1)} %fusion.5) | data formatting | bytes 1048576
  121.5 2.6 %fusion.6 = bf16[128,2048]{1,0:T(8,128)(2,1)} fusion(f32[128,2048]{1,0:T(8,128)S(1)} %fusion.46, bf16[2048,128]{1,0:T(8,128)(2,1)S(1)} %copy-done.1, f32[16,8,16,128]{3,2,1,0:T(8,128)} %bitcast.62, f32[128,128]{1,0:T(8,128)S(1)} %get-tuple-element.88), kind=kOutput, calls=%fused_computation.8 | convolution fusion | flops 68222976 | bytes 3211264 | tf_op jit(solution)/shard_map/dot_general | solution.py:139
  (31 shorter events, 0.3 us)
Async XLA Ops:
  7.2 21.8 %copy-start = (bf16[2048,128]{1,0:T(8,128)(2,1)S(1)}, bf16[2048,128]{1,0:T(8,128)(2,1)}, u32[]{:S(2)}) copy-start(bf16[2048,128]{1,0:T(8,128)(2,1)} %param.16) | copy-start | bytes 1572868
  7.2 25.2 %copy-start.10 = (bf16[896,128]{1,0:T(8,128)(2,1)S(1)}, bf16[896,128]{1,0:T(8,128)(2,1)}, u32[]{:S(2)}) copy-start(bf16[896,128]{1,0:T(8,128)(2,1)} %param.13) | copy-start | bytes 688132
  7.2 25.5 %copy-start.1 = (bf16[2048,128]{1,0:T(8,128)(2,1)S(1)}, bf16[2048,128]{1,0:T(8,128)(2,1)}, u32[]{:S(2)}) copy-start(bf16[2048,128]{1,0:T(8,128)(2,1)} %param.17) | copy-start | bytes 1572868
  9.5 31.6 %all-to-all-start = ((bf16[16,40,128]{2,1,0:T(8,128)(2,1)}), bf16[16,40,128]{2,1,0:T(8,128)(2,1)S(1)}, u32[]{:S(2)}, u32[]{:S(2)}) async-start(bf16[16,40,128]{2,1,0:T(8,128)(2,1)} %broadcast_in_dim.10), calls=%async_computation | async-start | bytes 327680 | tf_op jit(solution)/shard_map/all_to_all | solution.py:21
  28.9 77.9 %all-gather.3.cloned.1.call-start = ((), (), s32[]{:S(2)}) async-start(), calls=%async_computation.4 | async-start | bytes 1474560 | tf_op jit(solution)/shard_map/all_gather | solution.py:79
  29.0 3.7 %copy-start.2 = (bf16[896,2048]{1,0:T(8,128)(2,1)S(1)}, bf16[896,2048]{1,0:T(8,128)(2,1)}, u32[]{:S(2)}) copy-start(bf16[896,2048]{1,0:T(8,128)(2,1)} %param.15) | copy-start | bytes 11010052
  32.4 1.6 %copy-start.11 = (bf16[896,128]{1,0:T(8,128)(2,1)S(1)}, bf16[896,128]{1,0:T(8,128)(2,1)}, u32[]{:S(2)}) copy-start(bf16[896,128]{1,0:T(8,128)(2,1)} %param.14) | copy-start | bytes 688132
  32.7 73.5 %copy-start.6 = (f32[8,128]{1,0:T(8,128)S(1)}, f32[8,128]{1,0:T(8,128)}, u32[]{:S(2)}) copy-start(f32[8,128]{1,0:T(8,128)} %param.23) | copy-start | bytes 12292
  32.7 73.4 %copy-start.7 = (f32[8,128]{1,0:T(8,128)S(1)}, f32[8,128]{1,0:T(8,128)}, u32[]{:S(2)}) copy-start(f32[8,128]{1,0:T(8,128)} %param.22) | copy-start | bytes 12292
  32.7 73.4 %copy-start.8 = (f32[8,128]{1,0:T(8,128)S(1)}, f32[8,128]{1,0:T(8,128)}, u32[]{:S(2)}) copy-start(f32[8,128]{1,0:T(8,128)} %param.21) | copy-start | bytes 12292
  32.7 73.4 %copy-start.9 = (f32[8,128]{1,0:T(8,128)S(1)}, f32[8,128]{1,0:T(8,128)}, u32[]{:S(2)}) copy-start(f32[8,128]{1,0:T(8,128)} %param.20) | copy-start | bytes 12292
  41.1 0.7 copy-start.3
  86.1 18.7 %all-to-all-start.3 = ((bf16[64,8,128]{2,1,0:T(8,128)(2,1)}), bf16[64,8,128]{2,1,0:T(8,128)(2,1)S(1)}, u32[]{:S(2)}, u32[]{:S(2)}) async-start(bf16[64,8,128]{2,1,0:T(8,128)(2,1)} %bitcast.14), calls=%async_computation.3 | async-start | bytes 262144 | tf_op jit(solution)/shard_map/all_to_all | solution.py:21
  107.8 2.8 %copy-start.4 = (f32[128,128]{1,0:T(8,128)S(1)}, f32[128,128]{1,0:T(8,128)}, u32[]{:S(2)}) copy-start(f32[128,128]{1,0:T(8,128)} %param.18) | copy-start | bytes 196612
  109.3 2.1 %copy-start.5 = (f32[128,128]{1,0:T(8,128)S(1)}, f32[128,128]{1,0:T(8,128)}, u32[]{:S(2)}) copy-start(f32[128,128]{1,0:T(8,128)} %param.19) | copy-start | bytes 196612
Sparse Core Ops, SparseCore 0:
  41.9 40.1 all-gather.2

commit v2 on v0

v2 whole, which is shorter than its diff:
```python
import jax
import jax.numpy as jnp
from jax import lax
from jax.experimental import pallas as pl
from jax.experimental.pallas import tpu as pltpu
from jax.sharding import PartitionSpec as P


AW = 1024
RANK = 128


first_decay = 0.8
second_decay = 0.9
learning_rate = 0.02
norm_epsilon = 1e-06
f32 = jnp.float32
bf16 = jnp.bfloat16
contract_leading = (((0,), (0,)), ((), ()))
contract_trailing = (((1,), (1,)), ((), ()))


def exchange(chunks, axes):
    return lax.all_to_all(chunks, axes, 0, 0, tiled=True)


def split(array):
    upper = array.astype(bf16)
    return upper, (array - upper.astype(f32)).astype(bf16)


def moments(projected, first_old, second_old, clip_factor):
    scaled = clip_factor * projected
    first_new = first_decay * first_old + (1.0 - first_decay) * scaled
    second_new = second_decay * second_old + (1.0 - second_decay) * scaled * scaled
    return (first_new, second_new, first_new / jnp.sqrt(second_new))


def finish_kernel(
    fs_ref,
    rows_ref,
    wholes_ref,
    basis_value_ref,
    basis_output_ref,
    weight_value_ref,
    weight_output_ref,
    step_value_ref,
    step_output_ref,
    new_weight_value_ref,
    new_weight_output_ref,
    copy_value_ref,
    copy_output_ref,
    new_first_value_ref,
    new_second_value_ref,
    new_first_output_ref,
    new_second_output_ref,
    value_ref,
    output_ref,
):
    fs, _, columns = rows_ref.shape
    ranks = new_first_value_ref.shape[0]
    block = weight_value_ref.shape[0]
    cut = wholes_ref.shape[2] // 2
    total = rows_ref[0, 6 * ranks : 6 * ranks + 8, :]
    for i in range(1, fs):
        total = total + rows_ref[i, 6 * ranks : 6 * ranks + 8, :]
    mean_square = jnp.max(total, keepdims=True) / (2 * RANK * AW)
    clip_factor = jnp.minimum(1.0, 1.0 / jnp.sqrt(mean_square + norm_epsilon))

    def part(i, k):
        return rows_ref[i, k * ranks : (k + 1) * ranks, :]

    for i in range(fs):
        here = slice(i * ranks, (i + 1) * ranks)
        value_ref[here, :] = moments(part(i, 0), part(i, 2), part(i, 3), clip_factor)[2]
        output_ref[here, :] = moments(part(i, 1), part(i, 4), part(i, 5), clip_factor)[2]
    own = fs_ref[0]
    first, second, _ = moments(part(own, 0), part(own, 2), part(own, 3), clip_factor)
    new_first_value_ref[...] = first
    new_second_value_ref[...] = second
    first, second, _ = moments(part(own, 1), part(own, 4), part(own, 5), clip_factor)
    new_first_output_ref[...] = first
    new_second_output_ref[...] = second

    value_upper, value_lower = split(value_ref[...])
    output_upper, output_lower = split(output_ref[...].T)

    def value_step(basis):
        return jnp.dot(basis, value_upper, preferred_element_type=f32) + jnp.dot(
            basis, value_lower, preferred_element_type=f32
        )

    def output_step(basis):
        return lax.dot_general(
            output_upper, basis, contract_trailing, preferred_element_type=f32
        ) + lax.dot_general(output_lower, basis, contract_trailing, preferred_element_type=f32)

    own_rows = pl.ds(pl.multiple_of(own * block, block), block)
    step = value_step(basis_value_ref[own_rows, :])
    step_value_ref[...] = step
    new_weight_value_ref[...] = weight_value_ref[...] - learning_rate * step
    step = output_step(basis_output_ref[own_rows, :])
    step_output_ref[...] = step
    new_weight_output_ref[...] = weight_output_ref[...] - learning_rate * step
    for i in range(fs):
        here = slice(i * block, (i + 1) * block)
        whole = wholes_ref[:, i, :cut, :].reshape(block, columns).astype(f32)
        step = value_step(basis_value_ref[here, :])
        copy_value_ref[here, :] = (whole - learning_rate * step).astype(bf16)
        whole = wholes_ref[:, i, cut:, :].reshape(block, columns).astype(f32)
        step = output_step(basis_output_ref[here, :])
        copy_output_ref[:, here] = (whole - learning_rate * step).astype(bf16)


vmem = pl.BlockSpec(memory_space=pltpu.VMEM)
smem = pl.BlockSpec(memory_space=pltpu.SMEM)


def call(kernel, inputs, shapes, specs=None, scratch=(), flops=0, room=8, grid=None):
    outs = tuple(jax.ShapeDtypeStruct(s, t) for s, t in shapes)
    more = {} if grid is None else {"grid": grid}
    return pl.pallas_call(
        kernel,
        out_shape=outs,
        in_specs=[vmem] * len(inputs) if specs is None else specs,
        out_specs=tuple(vmem for _ in outs),
        scratch_shapes=scratch,
        compiler_params=pltpu.CompilerParams(vmem_limit_bytes=room * 2**20),
        cost_estimate=pl.CostEstimate(flops=flops, bytes_accessed=2**20, transcendentals=0),
        **more,
    )(*inputs)


def partial_kernel(
    rep_ref,
    hidden_ref,
    grad_value_ref,
    grad_output_ref,
    mixed_ref,
    basis_value_ref,
    basis_output_ref,
    weight_value_ref,
    weight_output_ref,
    out_ref,
    value_ref,
    output_ref,
):
    step = pl.program_id(0)

    @pl.when(step == 0)
    def _():
        value_ref[...] = jnp.zeros_like(value_ref)
        output_ref[...] = jnp.zeros_like(output_ref)

    for tokens_ref, basis_ref, other_ref, sum_ref in (
        (hidden_ref, basis_value_ref, grad_value_ref, value_ref),
        (grad_output_ref, basis_output_ref, mixed_ref, output_ref),
    ):
        reduced = jnp.dot(tokens_ref[...], basis_ref[...], preferred_element_type=f32)
        upper, lower = split(reduced)
        other = other_ref[...]
        sum_ref[...] += lax.dot_general(
            upper, other, contract_leading, preferred_element_type=f32
        ) + lax.dot_general(lower, other, contract_leading, preferred_element_type=f32)

    @pl.when(step == pl.num_programs(0) - 1)
    def _():
        fs, height, _ = out_ref.shape
        ranks = RANK // fs
        count = 2 * ranks
        cut = (height - 2 * count) // 2
        piece = pl.ds(pl.multiple_of(rep_ref[0] * cut, cut), cut)
        piece_value = weight_value_ref[piece, :].astype(bf16)
        piece_output = weight_output_ref[piece, :].astype(bf16)
        for i in range(fs):
            here = slice(i * ranks, (i + 1) * ranks)
            upper, lower = split(jnp.concatenate([value_ref[here, :], output_ref[here, :]]))
            out_ref[i, :count, :] = upper
            out_ref[i, count : 2 * count, :] = lower
            out_ref[i, 2 * count : 2 * count + cut, :] = piece_value
            out_ref[i, 2 * count + cut :, :] = piece_output


def partial(rep_index, hidden, grad_value, grad_output, mixed, bases, weights, fs, rep):
    tokens, depth = hidden.shape
    rows, columns = weights[0].shape
    steps = 4
    block = tokens // steps
    wide = pl.BlockSpec((block, depth), lambda i: (i, 0))
    narrow = pl.BlockSpec((block, columns), lambda i: (i, 0))
    height = 4 * (RANK // fs) + 2 * (rows // rep)
    return call(
        partial_kernel,
        (rep_index, hidden, grad_value, grad_output, mixed, *bases, *weights),
        [((fs, height, columns), bf16)],
        specs=[smem, wide, narrow, wide, narrow] + [vmem] * 4,
        scratch=[pltpu.VMEM((RANK, columns), f32)] * 2,
        flops=4 * tokens * depth * RANK,
        room=61,
        grid=(steps,),
    )[0]


def sum_kernel(mixed_ref, out_ref):
    count = out_ref.shape[1]
    total = mixed_ref[0, : 2 * count, :].astype(f32)
    for i in range(1, mixed_ref.shape[0]):
        total = total + mixed_ref[i, : 2 * count, :].astype(f32)
    total = total[:count] + total[count:]
    for j in range(out_ref.shape[0]):
        out_ref[j] = total


def squares_kernel(sums_ref, whole_ref, squares_ref):
    total = sums_ref[0]
    for j in range(1, sums_ref.shape[0]):
        total = total + sums_ref[j]
    whole_ref[...] = total
    squares = jnp.sum(total * total, keepdims=True)
    squares_ref[...] = jnp.broadcast_to(squares[None], squares_ref.shape)


def pack_kernel(whole_ref, first_value, second_value, first_output, second_output, sq_ref, out_ref):
    ranks = first_value.shape[0]
    out_ref[: 2 * ranks, :] = whole_ref[...]
    at = 2 * ranks
    for old_ref in (first_value, second_value, first_output, second_output):
        out_ref[at : at + ranks, :] = old_ref[...]
        at += ranks
    total = sq_ref[0]
    for t in range(1, sq_ref.shape[0]):
        total = total + sq_ref[t]
    out_ref[at:, :] = total


def local(
    saved_hidden,
    grad_value,
    saved_mixed,
    grad_output,
    basis_value,
    basis_output,
    weight_value,
    weight_output,
    first_value,
    second_value,
    first_output,
    second_output,
):
    fs, rep, tp = lax.axis_size("fs"), lax.axis_size("rep"), lax.axis_size("tp")
    fs_index = lax.axis_index("fs").astype(jnp.int32).reshape(1)
    rep_index = lax.axis_index("rep").astype(jnp.int32).reshape(1)
    rows, columns = weight_value.shape
    ranks = first_value.shape[0]

    start = partial(
        rep_index,
        saved_hidden,
        grad_value,
        grad_output,
        saved_mixed,
        (basis_value, basis_output),
        (weight_value, weight_output),
        fs,
        rep,
    )
    mixed = exchange(start, "fs")

    count = 2 * ranks
    summed = call(sum_kernel, (mixed,), [((rep, count, columns), f32)])[0]
    summed = exchange(summed, "rep")
    whole, squares = call(
        squares_kernel, (summed,), [((count, columns), f32), ((tp, 8, columns), f32)]
    )
    squares = exchange(squares, "tp")

    pieces = mixed[:, 2 * count :]
    wholes = exchange(jnp.broadcast_to(pieces[None], (rep, *pieces.shape)), "rep")
    packed = call(
        pack_kernel,
        (whole, first_value, second_value, first_output, second_output, squares),
        [((6 * ranks + 8, columns), f32)],
    )[0]
    gathered = lax.all_gather(packed, "fs")

    block, depth = rows, basis_value.shape[0]
    shapes = [((block, columns), f32)] * 4
    shapes += [((depth, columns), bf16), ((block, depth), bf16)] + [((ranks, columns), f32)] * 4
    return call(
        finish_kernel,
        (fs_index, gathered, wholes, basis_value, basis_output, weight_value, weight_output),
        shapes,
        specs=[smem] + [vmem] * 6,
        scratch=[pltpu.VMEM((RANK, columns), f32)] * 2,
        flops=8 * depth * RANK * columns,
        room=16,
    )


def solution(mesh):
    return jax.shard_map(
        local,
        mesh=mesh,
        in_specs=(
            P(("fs", "rep"), None),
            P(("fs", "rep"), "tp"),
            P(("fs", "rep"), "tp"),
            P(("fs", "rep"), None),
            P(),
            P(),
            P("fs", "tp"),
            P("tp", "fs"),
            P("fs", "tp"),
            P("fs", "tp"),
            P("fs", "tp"),
            P("fs", "tp"),
        ),
        out_specs=(
            P("fs", "tp"),
            P("tp", "fs"),
            P("fs", "tp"),
            P("tp", "fs"),
            P(None, "tp"),
            P("tp", None),
            P("fs", "tp"),
            P("fs", "tp"),
            P("fs", "tp"),
            P("fs", "tp"),
        ),
        check_vma=False,
    )
```

time: 357 us -> 111 us (0.31)
  the two profiles are of different devices: /device:TPU:6 before, /device:TPU:8 now
where the time goes in v2:
time: 111 us
  blocking collectives  83.8 us (75%)
  Pallas kernels  10.5 us (9%)
  starting transfers between devices  9.2 us (8%)
  waiting for transfers between devices  5.44 us (5%)
  local copies, waits for them, and re-layouts  1.21 us (1%)
    all_to_all x2, blocking collectives, exchange(): return lax.all_to_all(chunks, axes, 0, 0, tiled=True)  51.7 us
    all_gather x1, blocking collectives, local(): gathered = lax.all_gather(packed, 'fs')  32.2 us
    pallas_call x5, Pallas kernels, call(): pl.pallas_call(kernel, out_shape=outs, in_specs=[vmem] * len(inputs) if s...  10.5 us
    all_to_all x2, starting transfers between devices, exchange(): return lax.all_to_all(chunks, axes, 0, 0, tiled=True)  9.2 us
    all_to_all x2, waiting for transfers between devices, exchange(): return lax.all_to_all(chunks, axes, 0, 0, tiled=True)  5.44 us
  transfers between devices with their start and end apart: 2, of which 1 were waited for; matrix products, arithmetic and copies ran while one was open for 0% of the time, Pallas kernels for 0%

profile of v2, /device:TPU:8, one launch (start us, length us, event | category | flops | bytes accessed | tf_op | source)
XLA Modules:
  0.0 110.9 jit_solution(3365545749300001282)
XLA Ops:
  0.6 7.4 %shard_map.195 = bf16[16,64,128]{2,1,0:T(8,128)(2,1)} custom-call(s32[1]{0:T(128)} %bitcast.1.rep_ref, bf16[896,2048]{1,0:T(8,128)(2,1)} %hidden_ref.1, bf16[896,128]{1,0:T(8,128)(2,1)} %grad_value_ref.1, bf16[896,2048]{1,0:T(8,128)(2,1)} %grad_output_ref.1, bf16[896,128]{1,0:T(8,128)(2,1)} %mixed_ref.1, bf16[2048,128]{1,0:T(8,128)(2,1)} %basis_value_ref.3, ...), custom_call_target="tpu_custom_call" | custom-call | flops 939524096 | bytes 1048576 | tf_op jit(solution)/shard_map/pallas_call | solution.py:122
  8.1 0.0 copy-start.4
  8.1 0.0 copy-start.5
  8.1 0.0 copy-start.6
  8.1 0.0 copy-start.7
  8.1 0.0 copy-start
  8.1 0.0 copy-start.1
  8.2 0.0 copy-start.2
  8.2 0.0 copy-start.3
  8.2 37.4 %all_to_all.20.mixed_ref = bf16[16,64,128]{2,1,0:T(8,128)(2,1)S(1)} all-to-all(bf16[16,64,128]{2,1,0:T(8,128)(2,1)} %shard_map.195), channel_id=1, replica_groups=mesh['fs'=16,'rep'=8,'tp'=8] {'fs'}, dimensions={0} | all-to-all | bytes 524288 | tf_op jit(solution)/shard_map/all_to_all | solution.py:24
  45.6 14.3 %all_to_all.21.sums_ref = f32[8,16,128]{2,1,0:T(8,128)S(1)} all-to-all(f32[8,16,128]{2,1,0:T(8,128)S(1)} %shard_map.196), channel_id=1, replica_groups=mesh['fs'=16,'rep'=8,'tp'=8] {'rep'}, dimensions={0} | all-to-all | bytes 131072 | tf_op jit(solution)/shard_map/all_to_all | solution.py:24
  59.9 0.7 shard_map.197
  60.6 4.3 %all-to-all-start.2 = ((f32[8,8,128]{2,1,0:T(8,128)}), f32[8,8,128]{2,1,0:T(8,128)S(1)}, u32[]{:S(2)}, u32[]{:S(2)}) async-start(f32[8,8,128]{2,1,0:T(8,128)} %get-tuple-element.13), calls=%async_computation.2 | async-start | bytes 65536 | tf_op jit(solution)/shard_map/all_to_all | solution.py:24
  64.9 5.4 %all-to-all-done.2.sq_ref = f32[8,8,128]{2,1,0:T(8,128)S(1)} async-done(((f32[8,8,128]{2,1,0:T(8,128)}), f32[8,8,128]{2,1,0:T(8,128)S(1)}, u32[]{:S(2)}, u32[]{:S(2)}) %all-to-all-start.2) | async-done | bytes 32800 | tf_op jit(solution)/shard_map/all_to_all | solution.py:24
  70.4 1.2 %broadcast_in_dim.2 = bf16[8,16,32,128]{3,2,1,0:T(8,128)(2,1)} broadcast(bf16[16,32,128]{2,1,0:T(8,128)(2,1)S(1)} %slice.4), dimensions={1,2,3} | broadcast | bytes 1179648 | tf_op jit(solution)/shard_map/broadcast_in_dim | solution.py:278
  71.5 4.9 %all-to-all-start.3 = ((bf16[8,16,32,128]{3,2,1,0:T(8,128)(2,1)}), bf16[8,16,32,128]{3,2,1,0:T(8,128)(2,1)S(1)}, u32[]{:S(2)}, u32[]{:S(2)}) async-start(bf16[8,16,32,128]{3,2,1,0:T(8,128)(2,1)} %broadcast_in_dim.2), calls=%async_computation.3 | async-start | bytes 2097152 | tf_op jit(solution)/shard_map/all_to_all | solution.py:24
  76.4 0.0 copy-done.4
  76.4 0.0 copy-done.5
  76.4 0.0 copy-done.6
  76.4 0.0 copy-done.7
  76.5 32.2 %all-gather = f32[896,128]{1,0:T(8,128)S(1)} all-gather(f32[56,128]{1,0:T(8,128)S(1)} %shard_map.198), channel_id=2, replica_groups=mesh['fs'=16,'rep'=8,'tp'=8] {'fs'}, dimensions={0}, use_global_device_ids=true | all-gather | bytes 487424 | tf_op jit(solution)/shard_map/all_gather | solution.py:284
  108.6 0.0 all-to-all-done.3.wholes_ref
  108.6 0.0 copy-done
  108.6 0.0 copy-done.1
  108.6 0.0 copy-done.2
  108.6 0.0 copy-done.3
  108.7 2.3 %shard_map.199 = (f32[128,128]{1,0:T(8,128)}, f32[128,128]{1,0:T(8,128)}, f32[128,128]{1,0:T(8,128)}, f32[128,128]{1,0:T(8,128)}, bf16[2048,128]{1,0:T(8,128)(2,...) custom-call(s32[1]{0:T(128)} %bitcast.fs_ref, ...), custom_call_target="tpu_custom_call" | custom-call | flops 268435456 | bytes 1048576 | tf_op jit(solution)/shard_map/pallas_call | solution.py:122
  (3 shorter events, 0.0 us)
Async XLA Ops:
  8.1 68.3 %copy-start.4 = (f32[8,128]{1,0:T(8,128)S(1)}, f32[8,128]{1,0:T(8,128)}, u32[]{:S(2)}) copy-start(f32[8,128]{1,0:T(8,128)} %first_value.1) | copy-start | bytes 12292
  8.1 68.3 %copy-start.5 = (f32[8,128]{1,0:T(8,128)S(1)}, f32[8,128]{1,0:T(8,128)}, u32[]{:S(2)}) copy-start(f32[8,128]{1,0:T(8,128)} %second_value.1) | copy-start | bytes 12292
  8.1 68.3 %copy-start.6 = (f32[8,128]{1,0:T(8,128)S(1)}, f32[8,128]{1,0:T(8,128)}, u32[]{:S(2)}) copy-start(f32[8,128]{1,0:T(8,128)} %first_output.1) | copy-start | bytes 12292
  8.1 68.3 %copy-start.7 = (f32[8,128]{1,0:T(8,128)S(1)}, f32[8,128]{1,0:T(8,128)}, u32[]{:S(2)}) copy-start(f32[8,128]{1,0:T(8,128)} %second_output.1) | copy-start | bytes 12292
  8.1 100.5 %copy-start = (bf16[2048,128]{1,0:T(8,128)(2,1)S(1)}, bf16[2048,128]{1,0:T(8,128)(2,1)}, u32[]{:S(2)}) copy-start(bf16[2048,128]{1,0:T(8,128)(2,1)} %basis_value_ref.3) | copy-start | bytes 1572868
  8.1 100.5 %copy-start.1 = (bf16[2048,128]{1,0:T(8,128)(2,1)S(1)}, bf16[2048,128]{1,0:T(8,128)(2,1)}, u32[]{:S(2)}) copy-start(bf16[2048,128]{1,0:T(8,128)(2,1)} %basis_output_ref.3) | copy-start | bytes 1572868
  8.2 100.5 %copy-start.2 = (f32[128,128]{1,0:T(8,128)S(1)}, f32[128,128]{1,0:T(8,128)}, u32[]{:S(2)}) copy-start(f32[128,128]{1,0:T(8,128)} %weight_value_ref.3) | copy-start | bytes 196612
  8.2 100.5 %copy-start.3 = (f32[128,128]{1,0:T(8,128)S(1)}, f32[128,128]{1,0:T(8,128)}, u32[]{:S(2)}) copy-start(f32[128,128]{1,0:T(8,128)} %weight_output_ref.3) | copy-start | bytes 196612
  60.6 9.7 %all-to-all-start.2 = ((f32[8,8,128]{2,1,0:T(8,128)}), f32[8,8,128]{2,1,0:T(8,128)S(1)}, u32[]{:S(2)}, u32[]{:S(2)}) async-start(f32[8,8,128]{2,1,0:T(8,128)} %get-tuple-element.13), calls=%async_computation.2 | async-start | bytes 65536 | tf_op jit(solution)/shard_map/all_to_all | solution.py:24
  71.5 37.1 %all-to-all-start.3 = ((bf16[8,16,32,128]{3,2,1,0:T(8,128)(2,1)}), bf16[8,16,32,128]{3,2,1,0:T(8,128)(2,1)S(1)}, u32[]{:S(2)}, u32[]{:S(2)}) async-start(bf16[8,16,32,128]{3,2,1,0:T(8,128)(2,1)} %broadcast_in_dim.2), calls=%async_computation.3 | async-start | bytes 2097152 | tf_op jit(solution)/shard_map/all_to_all | solution.py:24

commit v3 on v2

--- a/solution.py
+++ b/solution.py
@@ -142,29 +142,38 @@
     weight_value_ref,
     weight_output_ref,
     out_ref,
-    value_ref,
-    output_ref,
+    hidden_sum_ref,
+    output_sum_ref,
 ):
     step = pl.program_id(0)
-
-    @pl.when(step == 0)
-    def _():
-        value_ref[...] = jnp.zeros_like(value_ref)
-        output_ref[...] = jnp.zeros_like(output_ref)
-
-    for tokens_ref, basis_ref, other_ref, sum_ref in (
-        (hidden_ref, basis_value_ref, grad_value_ref, value_ref),
-        (grad_output_ref, basis_output_ref, mixed_ref, output_ref),
+    for tokens_ref, basis_ref, sum_ref in (
+        (hidden_ref, basis_value_ref, hidden_sum_ref),
+        (grad_output_ref, basis_output_ref, output_sum_ref),
     ):
         reduced = jnp.dot(tokens_ref[...], basis_ref[...], preferred_element_type=f32)
-        upper, lower = split(reduced)
-        other = other_ref[...]
-        sum_ref[...] += lax.dot_general(
-            upper, other, contract_leading, preferred_element_type=f32
-        ) + lax.dot_general(lower, other, contract_leading, preferred_element_type=f32)
+
+        @pl.when(step == 0)
+        def _():
+            sum_ref[...] = reduced
+
+        @pl.when(step > 0)
+        def _():
+            sum_ref[...] += reduced
 
     @pl.when(step == pl.num_programs(0) - 1)
     def _():
+        products = []
+        for sum_ref, other_ref in (
+            (hidden_sum_ref, grad_value_ref),
+            (output_sum_ref, mixed_ref),
+        ):
+            upper, lower = split(sum_ref[...])
+            other = other_ref[...]
+            products.append(
+                lax.dot_general(upper, other, contract_leading, preferred_element_type=f32)
+                + lax.dot_general(lower, other, contract_leading, preferred_element_type=f32)
+            )
+        value, output = products
         fs, height, _ = out_ref.shape
         ranks = RANK // fs
         count = 2 * ranks
@@ -174,7 +183,7 @@
         piece_output = weight_output_ref[piece, :].astype(bf16)
         for i in range(fs):
             here = slice(i * ranks, (i + 1) * ranks)
-            upper, lower = split(jnp.concatenate([value_ref[here, :], output_ref[here, :]]))
+            upper, lower = split(jnp.concatenate([value[here], output[here]]))
             out_ref[i, :count, :] = upper
             out_ref[i, count : 2 * count, :] = lower
             out_ref[i, 2 * count : 2 * count + cut, :] = piece_value
@@ -185,16 +194,18 @@
     tokens, depth = hidden.shape
     rows, columns = weights[0].shape
     steps = 4
-    block = tokens // steps
-    wide = pl.BlockSpec((block, depth), lambda i: (i, 0))
-    narrow = pl.BlockSpec((block, columns), lambda i: (i, 0))
+    block = depth // steps
+    wide = pl.BlockSpec((tokens, block), lambda i: (0, i))
+    basis = pl.BlockSpec((block, RANK), lambda i: (i, 0))
+    narrow = pl.BlockSpec((tokens, columns), lambda i: (0, 0))
+    weight = pl.BlockSpec((rows, columns), lambda i: (0, 0))
     height = 4 * (RANK // fs) + 2 * (rows // rep)
     return call(
         partial_kernel,
         (rep_index, hidden, grad_value, grad_output, mixed, *bases, *weights),
         [((fs, height, columns), bf16)],
-        specs=[smem, wide, narrow, wide, narrow] + [vmem] * 4,
-        scratch=[pltpu.VMEM((RANK, columns), f32)] * 2,
+        specs=[smem, wide, narrow, wide, narrow, basis, basis, weight, weight],
+        scratch=[pltpu.VMEM((tokens, RANK), f32)] * 2,
         flops=4 * tokens * depth * RANK,
         room=61,
         grid=(steps,),
@@ -211,13 +222,17 @@
         out_ref[j] = total
 
 
-def squares_kernel(sums_ref, whole_ref, squares_ref):
+def squares_kernel(sums_ref, mixed_ref, whole_ref, squares_ref, spread_ref):
     total = sums_ref[0]
     for j in range(1, sums_ref.shape[0]):
         total = total + sums_ref[j]
     whole_ref[...] = total
     squares = jnp.sum(total * total, keepdims=True)
     squares_ref[...] = jnp.broadcast_to(squares[None], squares_ref.shape)
+    rep, _, height, _ = spread_ref.shape
+    pieces = mixed_ref[:, mixed_ref.shape[1] - height :, :]
+    for j in range(rep):
+        spread_ref[j] = pieces
 
 
 def pack_kernel(whole_ref, first_value, second_value, first_output, second_output, sq_ref, out_ref):
@@ -269,13 +284,19 @@
     count = 2 * ranks
     summed = call(sum_kernel, (mixed,), [((rep, count, columns), f32)])[0]
     summed = exchange(summed, "rep")
-    whole, squares = call(
-        squares_kernel, (summed,), [((count, columns), f32), ((tp, 8, columns), f32)]
+    height = mixed.shape[1] - 2 * count
+    whole, squares, spread = call(
+        squares_kernel,
+        (summed, mixed),
+        [
+            ((count, columns), f32),
+            ((tp, 8, columns), f32),
+            ((rep, fs, height, columns), bf16),
+        ],
     )
     squares = exchange(squares, "tp")
 
-    pieces = mixed[:, 2 * count :]
-    wholes = exchange(jnp.broadcast_to(pieces[None], (rep, *pieces.shape)), "rep")
+    wholes = exchange(spread, "rep")
     packed = call(
         pack_kernel,
         (whole, first_value, second_value, first_output, second_output, squares),

time: 111 us -> 112 us (level)
  blocking collectives: 83.8 us -> 93.3 us
  waiting for transfers between devices: 5.44 us -> 0.01 us
  starting transfers between devices: 9.2 us -> 4.92 us
  Pallas kernels: 10.5 us -> 12.1 us
  local copies, waits for them, and re-layouts: 1.21 us -> 0.04 us
    all_to_all x2 -> x3, blocking collectives: 51.7 us -> 61.2 us  [exchange(): return lax.all_to_all(chunks, axes, 0, 0, tiled=True)]
    all_to_all x2 -> x1, waiting for transfers between devices: 5.44 us -> 0.01 us  [exchange(): return lax.all_to_all(chunks, axes, 0, 0, tiled=True)]
    all_to_all x2 -> x1, starting transfers between devices: 9.2 us -> 4.92 us  [exchange(): return lax.all_to_all(chunks, axes, 0, 0, tiled=True)]
    pallas_call x5, Pallas kernels: 10.5 us -> 12.1 us  [call(): pl.pallas_call(kernel, out_shape=outs, in_specs=[vmem] * len(inputs) if s...]
    broadcast_in_dim x1 -> x0, local copies, waits for them, and re-layouts: 1.15 us -> none  [local(): jnp.broadcast_to(pieces[None], (rep, *pieces.shape))]
  transfers between devices with their start and end apart: 2 -> 1, of which waited for: 1 -> 0; matrix products, arithmetic and copies ran while one was open for 0% -> 0% of each run, Pallas kernels for 0% -> 0%
where the time goes in v3:
time: 112 us; the launch traced here: 111 us
  blocking collectives  93.3 us (83%)
  Pallas kernels  12.1 us (11%)
  starting transfers between devices  4.92 us (4%)
    all_to_all x3, blocking collectives, exchange(): return lax.all_to_all(chunks, axes, 0, 0, tiled=True)  61.2 us
    all_gather x1, blocking collectives, local(): gathered = lax.all_gather(packed, 'fs')  32.2 us
    pallas_call x5, Pallas kernels, call(): pl.pallas_call(kernel, out_shape=outs, in_specs=[vmem] * len(inputs) if s...  12.1 us
    all_to_all x1, starting transfers between devices, exchange(): return lax.all_to_all(chunks, axes, 0, 0, tiled=True)  4.92 us
  transfers between devices with their start and end apart: 1, of which 0 were waited for; matrix products, arithmetic and copies ran while one was open for 0% of the time, Pallas kernels for 0%

profile of v3, /device:TPU:8, one launch (start us, length us, event | category | flops | bytes accessed | tf_op | source)
XLA Modules:
  0.0 111.2 jit_solution(14705381096145634078)
XLA Ops:
  0.7 0.0 copy-start.4
  0.7 0.0 copy-start.5
  0.7 0.0 copy-start.6
  0.7 0.0 copy-start.7
  0.7 8.7 %shard_map.195 = bf16[16,64,128]{2,1,0:T(8,128)(2,1)} custom-call(s32[1]{0:T(128)} %bitcast.1.rep_ref, bf16[896,2048]{1,0:T(8,128)(2,1)} %hidden_ref.1, bf16[896,128]{1,0:T(8,128)(2,1)} %grad_value_ref.1, bf16[896,2048]{1,0:T(8,128)(2,1)} %grad_output_ref.1, bf16[896,128]{1,0:T(8,128)(2,1)} %mixed_ref.1, bf16[2048,128]{1,0:T(8,128)(2,1)} %basis_value_ref.3, ...), custom_call_target="tpu_custom_call" | custom-call | flops 939524096 | bytes 1048576 | tf_op jit(solution)/shard_map/pallas_call | solution.py:122
  9.4 0.0 copy-start
  9.4 0.0 copy-start.1
  9.4 0.0 copy-start.2
  9.4 0.0 copy-start.3
  9.4 37.4 %all_to_all.20.mixed_ref = bf16[16,64,128]{2,1,0:T(8,128)(2,1)S(1)} all-to-all(bf16[16,64,128]{2,1,0:T(8,128)(2,1)} %shard_map.195), channel_id=1, replica_groups=mesh['fs'=16,'rep'=8,'tp'=8] {'fs'}, dimensions={0} | all-to-all | bytes 524288 | tf_op jit(solution)/shard_map/all_to_all | solution.py:24
  46.8 14.3 %all_to_all.21.sums_ref = f32[8,16,128]{2,1,0:T(8,128)S(1)} all-to-all(f32[8,16,128]{2,1,0:T(8,128)S(1)} %shard_map.196), channel_id=1, replica_groups=mesh['fs'=16,'rep'=8,'tp'=8] {'rep'}, dimensions={0} | all-to-all | bytes 131072 | tf_op jit(solution)/shard_map/all_to_all | solution.py:24
  61.1 1.1 %shard_map.197 = (f32[16,128]{1,0:T(8,128)S(1)}, f32[8,8,128]{2,1,0:T(8,128)S(1)}, bf16[8,16,32,128]{3,2,1,0:T(8,128)(2,1)}) custom-call(f32[8,16,128]{2,1,0:T(8,128)S(1)} %all_to_all.21.sums_ref, bf16[16,64,128]{2,1,0:T(8,128)(2,1)S(1)} %all_to_all.20.mixed_ref), custom_call_target="tpu_custom_call" | custom-call | bytes 1048576 | tf_op jit(solution)/shard_map/pallas_call | solution.py:122
  62.2 9.5 %all_to_all.22.sq_ref = f32[8,8,128]{2,1,0:T(8,128)S(1)} all-to-all(f32[8,8,128]{2,1,0:T(8,128)S(1)} %get-tuple-element.14), channel_id=1, replica_groups=mesh['fs'=16,'rep'=8,'tp'=8] {'tp'}, dimensions={0} | all-to-all | bytes 65536 | tf_op jit(solution)/shard_map/all_to_all | solution.py:24
  71.7 4.9 %all-to-all-start.3 = ((bf16[8,16,32,128]{3,2,1,0:T(8,128)(2,1)}), bf16[8,16,32,128]{3,2,1,0:T(8,128)(2,1)S(1)}, u32[]{:S(2)}, u32[]{:S(2)}) async-start(bf16[8,16,32,128]{3,2,1,0:T(8,128)(2,1)} %get-tuple-element.15), calls=%async_computation.3 | async-start | bytes 2097152 | tf_op jit(solution)/shard_map/all_to_all | solution.py:24
  76.6 0.0 copy-done.4
  76.6 0.0 copy-done.5
  76.6 0.0 copy-done.6
  76.7 0.0 copy-done.7
  76.7 32.2 %all-gather = f32[896,128]{1,0:T(8,128)S(1)} all-gather(f32[56,128]{1,0:T(8,128)S(1)} %shard_map.198), channel_id=2, replica_groups=mesh['fs'=16,'rep'=8,'tp'=8] {'fs'}, dimensions={0}, use_global_device_ids=true | all-gather | bytes 487424 | tf_op jit(solution)/shard_map/all_gather | solution.py:305
  108.8 0.0 all-to-all-done.3.wholes_ref
  108.8 0.0 copy-done
  108.8 0.0 copy-done.1
  108.8 0.0 copy-done.2
  108.9 0.0 copy-done.3
  108.9 2.3 %shard_map.199 = (f32[128,128]{1,0:T(8,128)}, f32[128,128]{1,0:T(8,128)}, f32[128,128]{1,0:T(8,128)}, f32[128,128]{1,0:T(8,128)}, bf16[2048,128]{1,0:T(8,128)(2,...) custom-call(s32[1]{0:T(128)} %bitcast.fs_ref, ...), custom_call_target="tpu_custom_call" | custom-call | flops 268435456 | bytes 1048576 | tf_op jit(solution)/shard_map/pallas_call | solution.py:122
  (2 shorter events, 0.0 us)
Async XLA Ops:
  0.7 76.0 %copy-start.4 = (f32[8,128]{1,0:T(8,128)S(1)}, f32[8,128]{1,0:T(8,128)}, u32[]{:S(2)}) copy-start(f32[8,128]{1,0:T(8,128)} %first_value.1) | copy-start | bytes 12292
  0.7 76.0 %copy-start.5 = (f32[8,128]{1,0:T(8,128)S(1)}, f32[8,128]{1,0:T(8,128)}, u32[]{:S(2)}) copy-start(f32[8,128]{1,0:T(8,128)} %second_value.1) | copy-start | bytes 12292
  0.7 76.0 %copy-start.6 = (f32[8,128]{1,0:T(8,128)S(1)}, f32[8,128]{1,0:T(8,128)}, u32[]{:S(2)}) copy-start(f32[8,128]{1,0:T(8,128)} %first_output.1) | copy-start | bytes 12292
  0.7 76.0 %copy-start.7 = (f32[8,128]{1,0:T(8,128)S(1)}, f32[8,128]{1,0:T(8,128)}, u32[]{:S(2)}) copy-start(f32[8,128]{1,0:T(8,128)} %second_output.1) | copy-start | bytes 12292
  9.4 99.5 %copy-start = (bf16[2048,128]{1,0:T(8,128)(2,1)S(1)}, bf16[2048,128]{1,0:T(8,128)(2,1)}, u32[]{:S(2)}) copy-start(bf16[2048,128]{1,0:T(8,128)(2,1)} %basis_value_ref.3) | copy-start | bytes 1572868
  9.4 99.5 %copy-start.1 = (bf16[2048,128]{1,0:T(8,128)(2,1)S(1)}, bf16[2048,128]{1,0:T(8,128)(2,1)}, u32[]{:S(2)}) copy-start(bf16[2048,128]{1,0:T(8,128)(2,1)} %basis_output_ref.3) | copy-start | bytes 1572868
  9.4 99.5 %copy-start.2 = (f32[128,128]{1,0:T(8,128)S(1)}, f32[128,128]{1,0:T(8,128)}, u32[]{:S(2)}) copy-start(f32[128,128]{1,0:T(8,128)} %weight_value_ref.3) | copy-start | bytes 196612
  9.4 99.5 %copy-start.3 = (f32[128,128]{1,0:T(8,128)S(1)}, f32[128,128]{1,0:T(8,128)}, u32[]{:S(2)}) copy-start(f32[128,128]{1,0:T(8,128)} %weight_output_ref.3) | copy-start | bytes 196612
  71.7 37.1 %all-to-all-start.3 = ((bf16[8,16,32,128]{3,2,1,0:T(8,128)(2,1)}), bf16[8,16,32,128]{3,2,1,0:T(8,128)(2,1)S(1)}, u32[]{:S(2)}, u32[]{:S(2)}) async-start(bf16[8,16,32,128]{3,2,1,0:T(8,128)(2,1)} %get-tuple-element.15), calls=%async_computation.3 | async-start | bytes 2097152 | tf_op jit(solution)/shard_map/all_to_all | solution.py:24

commit v4 on v3

--- a/solution.py
+++ b/solution.py
@@ -38,47 +38,78 @@
 
 def finish_kernel(
     fs_ref,
+    rep_ref,
     rows_ref,
-    wholes_ref,
+    whole_ref,
+    first_value_ref,
+    second_value_ref,
+    first_output_ref,
+    second_output_ref,
     basis_value_ref,
     basis_output_ref,
     weight_value_ref,
     weight_output_ref,
-    step_value_ref,
-    step_output_ref,
-    new_weight_value_ref,
-    new_weight_output_ref,
-    copy_value_ref,
-    copy_output_ref,
-    new_first_value_ref,
-    new_second_value_ref,
-    new_first_output_ref,
-    new_second_output_ref,
-    value_ref,
-    output_ref,
+    *refs,
 ):
-    fs, _, columns = rows_ref.shape
-    ranks = new_first_value_ref.shape[0]
+    rep = len(refs) - 14
+    piece_refs, refs = refs[:rep], refs[rep:]
+    (
+        step_value_ref,
+        step_output_ref,
+        new_weight_value_ref,
+        new_weight_output_ref,
+        copy_value_ref,
+        copy_output_ref,
+        new_first_value_ref,
+        new_second_value_ref,
+        new_first_output_ref,
+        new_second_output_ref,
+        wholes_ref,
+        olds_ref,
+        value_ref,
+        output_ref,
+    ) = refs
+    fs, height, columns = rows_ref.shape
+    ranks = first_value_ref.shape[0]
+    count = 2 * ranks
     block = weight_value_ref.shape[0]
-    cut = wholes_ref.shape[2] // 2
-    total = rows_ref[0, 6 * ranks : 6 * ranks + 8, :]
+    cut = block // rep
+    part = 4 * ranks // rep
+    run = min(part, ranks)
+    for away in range(rep):
+        other = lax.rem(rep_ref[0] + away, rep)
+        wholes_ref[other] = piece_refs[away][:, : 2 * cut, :]
+        old = piece_refs[away][:, 2 * cut :, :].astype(f32)
+        olds_ref[other] = old[:, :part] + old[:, part:]
+
+    half = (height - count) // 2
+    total = rows_ref[0, count:, :].astype(f32)
     for i in range(1, fs):
-        total = total + rows_ref[i, 6 * ranks : 6 * ranks + 8, :]
+        total = total + rows_ref[i, count:, :].astype(f32)
+    total = total[:half] + total[half:]
     mean_square = jnp.max(total, keepdims=True) / (2 * RANK * AW)
     clip_factor = jnp.minimum(1.0, 1.0 / jnp.sqrt(mean_square + norm_epsilon))
 
-    def part(i, k):
-        return rows_ref[i, k * ranks : (k + 1) * ranks, :]
+    def old(i, k):
+        runs = [
+            olds_ref[at // part, i, at % part : at % part + run, :]
+            for at in range(k * ranks, (k + 1) * ranks, run)
+        ]
+        return jnp.concatenate(runs) if len(runs) > 1 else runs[0]
 
     for i in range(fs):
         here = slice(i * ranks, (i + 1) * ranks)
-        value_ref[here, :] = moments(part(i, 0), part(i, 2), part(i, 3), clip_factor)[2]
-        output_ref[here, :] = moments(part(i, 1), part(i, 4), part(i, 5), clip_factor)[2]
-    own = fs_ref[0]
-    first, second, _ = moments(part(own, 0), part(own, 2), part(own, 3), clip_factor)
+        row = rows_ref[i, :count, :].astype(f32)
+        value_ref[here, :] = moments(row[:ranks], old(i, 0), old(i, 1), clip_factor)[2]
+        output_ref[here, :] = moments(row[ranks:], old(i, 2), old(i, 3), clip_factor)[2]
+    first, second, _ = moments(
+        whole_ref[:ranks, :], first_value_ref[...], second_value_ref[...], clip_factor
+    )
     new_first_value_ref[...] = first
     new_second_value_ref[...] = second
-    first, second, _ = moments(part(own, 1), part(own, 4), part(own, 5), clip_factor)
+    first, second, _ = moments(
+        whole_ref[ranks:, :], first_output_ref[...], second_output_ref[...], clip_factor
+    )
     new_first_output_ref[...] = first
     new_second_output_ref[...] = second
 
@@ -95,6 +126,7 @@
             output_upper, basis, contract_trailing, preferred_element_type=f32
         ) + lax.dot_general(output_lower, basis, contract_trailing, preferred_element_type=f32)
 
+    own = fs_ref[0]
     own_rows = pl.ds(pl.multiple_of(own * block, block), block)
     step = value_step(basis_value_ref[own_rows, :])
     step_value_ref[...] = step
@@ -141,9 +173,14 @@
     basis_output_ref,
     weight_value_ref,
     weight_output_ref,
+    first_value_ref,
+    second_value_ref,
+    first_output_ref,
+    second_output_ref,
     out_ref,
     hidden_sum_ref,
     output_sum_ref,
+    old_ref,
 ):
     step = pl.program_id(0)
     for tokens_ref, basis_ref, sum_ref in (
@@ -174,45 +211,63 @@
                 + lax.dot_general(lower, other, contract_leading, preferred_element_type=f32)
             )
         value, output = products
-        fs, height, _ = out_ref.shape
-        ranks = RANK // fs
+        fs = out_ref.shape[0]
+        ranks, _ = first_value_ref.shape
         count = 2 * ranks
-        cut = (height - 2 * count) // 2
-        piece = pl.ds(pl.multiple_of(rep_ref[0] * cut, cut), cut)
+        rep, part, _ = old_ref.shape
+        cut = weight_value_ref.shape[0] // rep
+        run = min(part, ranks)
+        olds = (first_value_ref, second_value_ref, first_output_ref, second_output_ref)
+        for at in range(0, 4 * ranks, run):
+            from_row, to_row = at % ranks, at % part
+            old_ref[at // part, to_row : to_row + run, :] = olds[at // ranks][
+                from_row : from_row + run, :
+            ]
+        me = rep_ref[0]
+        piece = pl.ds(pl.multiple_of(me * cut, cut), cut)
         piece_value = weight_value_ref[piece, :].astype(bf16)
         piece_output = weight_output_ref[piece, :].astype(bf16)
+        old = old_ref[me]
+        upper = old.astype(bf16).astype(f32)
+        piece_old = jnp.concatenate([upper, old - upper]).astype(bf16)
+        weights_at = 2 * count
+        olds_at = weights_at + 2 * cut
         for i in range(fs):
             here = slice(i * ranks, (i + 1) * ranks)
             upper, lower = split(jnp.concatenate([value[here], output[here]]))
             out_ref[i, :count, :] = upper
-            out_ref[i, count : 2 * count, :] = lower
-            out_ref[i, 2 * count : 2 * count + cut, :] = piece_value
-            out_ref[i, 2 * count + cut :, :] = piece_output
-
-
-def partial(rep_index, hidden, grad_value, grad_output, mixed, bases, weights, fs, rep):
+            out_ref[i, count:weights_at, :] = lower
+            out_ref[i, weights_at : weights_at + cut, :] = piece_value
+            out_ref[i, weights_at + cut : olds_at, :] = piece_output
+            out_ref[i, olds_at:, :] = piece_old
+
+
+def partial(rep_index, hidden, grad_value, grad_output, mixed, bases, weights, olds, fs, rep):
     tokens, depth = hidden.shape
     rows, columns = weights[0].shape
+    ranks = olds[0].shape[0]
+    part = 4 * ranks // rep
     steps = 4
     block = depth // steps
     wide = pl.BlockSpec((tokens, block), lambda i: (0, i))
     basis = pl.BlockSpec((block, RANK), lambda i: (i, 0))
     narrow = pl.BlockSpec((tokens, columns), lambda i: (0, 0))
     weight = pl.BlockSpec((rows, columns), lambda i: (0, 0))
-    height = 4 * (RANK // fs) + 2 * (rows // rep)
+    old = pl.BlockSpec((ranks, columns), lambda i: (0, 0))
+    height = 4 * ranks + 2 * (rows // rep) + 2 * part
     return call(
         partial_kernel,
-        (rep_index, hidden, grad_value, grad_output, mixed, *bases, *weights),
+        (rep_index, hidden, grad_value, grad_output, mixed, *bases, *weights, *olds),
         [((fs, height, columns), bf16)],
-        specs=[smem, wide, narrow, wide, narrow, basis, basis, weight, weight],
-        scratch=[pltpu.VMEM((tokens, RANK), f32)] * 2,
+        specs=[smem, wide, narrow, wide, narrow, basis, basis, weight, weight] + [old] * 4,
+        scratch=[pltpu.VMEM((tokens, RANK), f32)] * 2 + [pltpu.VMEM((rep, part, columns), f32)],
         flops=4 * tokens * depth * RANK,
         room=61,
         grid=(steps,),
     )[0]
 
 
-def sum_kernel(mixed_ref, out_ref):
+def sum_kernel(mixed_ref, out_ref, pieces_ref):
     count = out_ref.shape[1]
     total = mixed_ref[0, : 2 * count, :].astype(f32)
     for i in range(1, mixed_ref.shape[0]):
@@ -220,32 +275,30 @@
     total = total[:count] + total[count:]
     for j in range(out_ref.shape[0]):
         out_ref[j] = total
-
-
-def squares_kernel(sums_ref, mixed_ref, whole_ref, squares_ref, spread_ref):
+    pieces_ref[...] = mixed_ref[:, 2 * count :, :]
+
+
+def squares_kernel(sums_ref, whole_ref, squares_ref):
     total = sums_ref[0]
     for j in range(1, sums_ref.shape[0]):
         total = total + sums_ref[j]
     whole_ref[...] = total
     squares = jnp.sum(total * total, keepdims=True)
     squares_ref[...] = jnp.broadcast_to(squares[None], squares_ref.shape)
-    rep, _, height, _ = spread_ref.shape
-    pieces = mixed_ref[:, mixed_ref.shape[1] - height :, :]
-    for j in range(rep):
-        spread_ref[j] = pieces
-
-
-def pack_kernel(whole_ref, first_value, second_value, first_output, second_output, sq_ref, out_ref):
-    ranks = first_value.shape[0]
-    out_ref[: 2 * ranks, :] = whole_ref[...]
-    at = 2 * ranks
-    for old_ref in (first_value, second_value, first_output, second_output):
-        out_ref[at : at + ranks, :] = old_ref[...]
-        at += ranks
-    total = sq_ref[0]
-    for t in range(1, sq_ref.shape[0]):
-        total = total + sq_ref[t]
-    out_ref[at:, :] = total
+
+
+def rows_kernel(whole_ref, squares_ref, out_ref):
+    count = whole_ref.shape[0]
+    total = squares_ref[0]
+    for t in range(1, squares_ref.shape[0]):
+        total = total + squares_ref[t]
+    total = total[:4]
+    upper = total.astype(bf16).astype(f32)
+    total = jnp.concatenate([upper, total - upper]).astype(bf16)
+    whole = whole_ref[...].astype(bf16)
+    for i in range(out_ref.shape[0]):
+        out_ref[i, :count, :] = whole
+        out_ref[i, count:, :] = total
 
 
 def local(
@@ -268,51 +321,60 @@
     rows, columns = weight_value.shape
     ranks = first_value.shape[0]
 
+    olds = (first_value, second_value, first_output, second_output)
+    weights = (weight_value, weight_output)
+    bases = (basis_value, basis_output)
     start = partial(
         rep_index,
         saved_hidden,
         grad_value,
         grad_output,
         saved_mixed,
-        (basis_value, basis_output),
-        (weight_value, weight_output),
+        bases,
+        weights,
+        olds,
         fs,
         rep,
     )
     mixed = exchange(start, "fs")
 
     count = 2 * ranks
-    summed = call(sum_kernel, (mixed,), [((rep, count, columns), f32)])[0]
+    height = mixed.shape[1] - 2 * count
+    summed, piece = call(
+        sum_kernel,
+        (mixed,),
+        [((rep, count, columns), f32), ((fs, height, columns), bf16)],
+    )
     summed = exchange(summed, "rep")
-    height = mixed.shape[1] - 2 * count
-    whole, squares, spread = call(
-        squares_kernel,
-        (summed, mixed),
-        [
-            ((count, columns), f32),
-            ((tp, 8, columns), f32),
-            ((rep, fs, height, columns), bf16),
-        ],
+    whole, squares = call(
+        squares_kernel, (summed,), [((count, columns), f32), ((tp, 8, columns), f32)]
     )
     squares = exchange(squares, "tp")
-
-    wholes = exchange(spread, "rep")
-    packed = call(
-        pack_kernel,
-        (whole, first_value, second_value, first_output, second_output, squares),
-        [((6 * ranks + 8, columns), f32)],
-    )[0]
-    gathered = lax.all_gather(packed, "fs")
-
-    block, depth = rows, basis_value.shape[0]
-    shapes = [((block, columns), f32)] * 4
-    shapes += [((depth, columns), bf16), ((block, depth), bf16)] + [((ranks, columns), f32)] * 4
+    rowed = call(rows_kernel, (whole, squares), [((fs, count + 8, columns), bf16)])[0]
+    gathered = exchange(rowed, "fs")
+
+    pieces = [piece] + [None] * (rep - 1)
+    up = down = piece
+    for far in range(1, rep // 2 + 1):
+        up = lax.ppermute(up, "rep", [(r, (r + 1) % rep) for r in range(rep)])
+        pieces[rep - far] = up
+        if 2 * far < rep:
+            down = lax.ppermute(down, "rep", [(r, (r - 1) % rep) for r in range(rep)])
+            pieces[far] = down
+
+    depth = basis_value.shape[0]
+    shapes = [((rows, columns), f32)] * 4
+    shapes += [((depth, columns), bf16), ((rows, depth), bf16)] + [((ranks, columns), f32)] * 4
     return call(
         finish_kernel,
-        (fs_index, gathered, wholes, basis_value, basis_output, weight_value, weight_output),
+        (fs_index, rep_index, gathered, whole, *olds, *bases, *weights, *pieces),
         shapes,
-        specs=[smem] + [vmem] * 6,
-        scratch=[pltpu.VMEM((RANK, columns), f32)] * 2,
+        specs=[smem] * 2 + [vmem] * (10 + rep),
+        scratch=[
+            pltpu.VMEM((rep, fs, 2 * (rows // rep), columns), bf16),
+            pltpu.VMEM((rep, fs, 4 * ranks // rep, columns), f32),
+        ]
+        + [pltpu.VMEM((RANK, columns), f32)] * 2,
         flops=8 * depth * RANK * columns,
         room=16,
     )

time: 112 us -> 106 us (0.946)
  the two profiles are of different devices: /device:TPU:8 before, /device:TPU:6 now
where the time goes in v4:
time: 106 us; the launch traced here: 105 us
  blocking collectives  46.2 us (44%)
  starting transfers between devices  35.8 us (34%)
  Pallas kernels  12.6 us (12%)
  waiting for transfers between devices  9.35 us (9%)
    all_to_all x2, blocking collectives, exchange(): return lax.all_to_all(chunks, axes, 0, 0, tiled=True)  46.2 us
    ppermute x3, starting transfers between devices, local(): down = lax.ppermute(down, 'rep', [(r, (r - 1) % rep) for r in range(rep)])  13.8 us
    pallas_call x5, Pallas kernels, call(): pl.pallas_call(kernel, out_shape=outs, in_specs=[vmem] * len(inputs) if s...  12.6 us
    all_to_all x2, starting transfers between devices, exchange(): return lax.all_to_all(chunks, axes, 0, 0, tiled=True)  12.5 us
    ppermute x4, starting transfers between devices, local(): up = lax.ppermute(up, 'rep', [(r, (r + 1) % rep) for r in range(rep)])  9.41 us
    ppermute x4, waiting for transfers between devices, local(): up = lax.ppermute(up, 'rep', [(r, (r + 1) % rep) for r in range(rep)])  5.62 us
    ppermute x3, waiting for transfers between devices, local(): down = lax.ppermute(down, 'rep', [(r, (r - 1) % rep) for r in range(rep)])  2.5 us
  transfers between devices with their start and end apart: 9, of which 4 were waited for; matrix products, arithmetic and copies ran while one was open for 0% of the time, Pallas kernels for 1%

profile of v4, /device:TPU:6, one launch (start us, length us, event | category | flops | bytes accessed | tf_op | source)
XLA Modules:
  0.0 104.8 jit_solution(3634825946363862295)
XLA Ops:
  0.7 0.0 copy-start
  0.7 0.0 copy-start.1
  0.7 0.0 copy-start.2
  0.7 0.0 copy-start.3
  0.7 0.0 copy-start.4
  0.7 0.0 copy-start.5
  0.7 0.0 copy-start.6
  0.7 0.0 copy-start.7
  0.7 8.8 %shard_map.195 = bf16[16,72,128]{2,1,0:T(8,128)(2,1)} custom-call(s32[1]{0:T(128)} %bitcast.1.rep_ref, bf16[896,2048]{1,0:T(8,128)(2,1)} %hidden_ref.1, bf16[896,128]{1,0:T(8,128)(2,1)} %grad_value_ref.1, bf16[896,2048]{1,0:T(8,128)(2,1)} %grad_output_ref.1, bf16[896,128]{1,0:T(8,128)(2,1)} %mixed_ref.1, bf16[2048,128]{1,0:T(8,128)(2,1)} %basis_value_ref.3, ...), custom_call_target="tpu_custom_call" | custom-call | flops 939524096 | bytes 1048576 | tf_op jit(solution)/shard_map/pallas_call | solution.py:154
  9.5 38.3 %all_to_all.20.mixed_ref = bf16[16,72,128]{2,1,0:T(8,128)(2,1)S(1)} all-to-all(bf16[16,72,128]{2,1,0:T(8,128)(2,1)} %shard_map.195), channel_id=1, replica_groups=mesh['fs'=16,'rep'=8,'tp'=8] {'fs'}, dimensions={0} | all-to-all | bytes 589824 | tf_op jit(solution)/shard_map/all_to_all | solution.py:24
  47.8 0.7 shard_map.196
  48.4 3.5 %collective-permute-start.3 = (bf16[16,40,128]{2,1,0:T(8,128)(2,1)S(1)}, bf16[16,40,128]{2,1,0:T(8,128)(2,1)S(1)}, u32[]{:S(2)}, u32[]{:S(2)}) collective-permute-start(bf16[16,40,128]{2,1,0:T(8,128)(2,1)S(1)} %get-tuple-element.17.refs_0_), channel_id=1, source_target_pairs={{0,8},{8,16},{16,24},{24,32},{32,40},{40,48},{48,56},{56,0},{1,9},... | collective-permute-start | bytes 491528 | tf_op jit(solution)/shard_map/ppermute | solution.py:359
  51.9 6.2 %all-to-all-start.1 = ((f32[8,16,128]{2,1,0:T(8,128)}), f32[8,16,128]{2,1,0:T(8,128)S(1)}, u32[]{:S(2)}, u32[]{:S(2)}) async-start(f32[8,16,128]{2,1,0:T(8,128)} %get-tuple-element.14), calls=%async_computation.1 | async-start | bytes 131072 | tf_op jit(solution)/shard_map/all_to_all | solution.py:24
  58.1 5.1 %collective-permute-start = (bf16[16,40,128]{2,1,0:T(8,128)(2,1)S(1)}, bf16[16,40,128]{2,1,0:T(8,128)(2,1)S(1)}, u32[]{:S(2)}, u32[]{:S(2)}) collective-permute-start(bf16[16,40,128]{2,1,0:T(8,128)(2,1)S(1)} %get-tuple-element.17.refs_0_), channel_id=1, source_target_pairs={{0,56},{8,0},{16,8},{24,16},{32,24},{40,32},{48,40},{56,48},{1,57}... | collective-permute-start | bytes 491528 | tf_op jit(solution)/shard_map/ppermute | solution.py:362
  63.3 0.0 collective-permute-done.3.refs_7_
  63.3 1.9 %collective-permute-start.4 = (bf16[16,40,128]{2,1,0:T(8,128)(2,1)S(1)}, bf16[16,40,128]{2,1,0:T(8,128)(2,1)S(1)}, u32[]{:S(2)}, u32[]{:S(2)}) collective-permute-start(bf16[16,40,128]{2,1,0:T(8,128)(2,1)S(1)} %collective-permute-done.3.refs_7_), channel_id=1, source_target_pairs={{0,8},{8,16},{16,24},{24,32},{32,40},{40,48},{48,56},{56,0},{1,9},... | collective-permute-start | bytes 491528 | tf_op jit(solution)/shard_map/ppermute | solution.py:359
  65.2 1.2 %all-to-all-done.1.sums_ref = f32[8,16,128]{2,1,0:T(8,128)S(1)} async-done(((f32[8,16,128]{2,1,0:T(8,128)}), f32[8,16,128]{2,1,0:T(8,128)S(1)}, u32[]{:S(2)}, u32[]{:S(2)}) %all-to-all-start.1) | async-done | bytes 65568 | tf_op jit(solution)/shard_map/all_to_all | solution.py:24
  66.4 0.1 shard_map.197
  66.6 8.0 %all_to_all.21.squares_ref = f32[8,8,128]{2,1,0:T(8,128)S(1)} all-to-all(f32[8,8,128]{2,1,0:T(8,128)S(1)} %get-tuple-element.16), channel_id=1, replica_groups=mesh['fs'=16,'rep'=8,'tp'=8] {'tp'}, dimensions={0} | all-to-all | bytes 65536 | tf_op jit(solution)/shard_map/all_to_all | solution.py:24
  74.5 0.7 shard_map.198
  75.2 6.3 %all-to-all-start.3 = ((bf16[16,24,128]{2,1,0:T(8,128)(2,1)}), bf16[16,24,128]{2,1,0:T(8,128)(2,1)S(1)}, u32[]{:S(2)}, u32[]{:S(2)}) async-start(bf16[16,24,128]{2,1,0:T(8,128)(2,1)} %shard_map.198), calls=%async_computation.3 | async-start | bytes 196608 | tf_op jit(solution)/shard_map/all_to_all | solution.py:24
  81.5 0.0 collective-permute-done.refs_1_
  81.5 3.7 %collective-permute-start.1 = (bf16[16,40,128]{2,1,0:T(8,128)(2,1)S(1)}, bf16[16,40,128]{2,1,0:T(8,128)(2,1)S(1)}, u32[]{:S(2)}, u32[]{:S(2)}) collective-permute-start(bf16[16,40,128]{2,1,0:T(8,128)(2,1)S(1)} %collective-permute-done.refs_1_), channel_id=1, source_target_pairs={{0,56},{8,0},{16,8},{24,16},{32,24},{40,32},{48,40},{56,48},{1,57}... | collective-permute-start | bytes 491528 | tf_op jit(solution)/shard_map/ppermute | solution.py:362
  85.3 0.0 collective-permute-done.4.refs_6_
  85.3 2.1 %collective-permute-start.5 = (bf16[16,40,128]{2,1,0:T(8,128)(2,1)S(1)}, bf16[16,40,128]{2,1,0:T(8,128)(2,1)S(1)}, u32[]{:S(2)}, u32[]{:S(2)}) collective-permute-start(bf16[16,40,128]{2,1,0:T(8,128)(2,1)S(1)} %collective-permute-done.4.refs_6_), channel_id=1, source_target_pairs={{0,8},{8,16},{16,24},{24,32},{32,40},{40,48},{48,56},{56,0},{1,9},... | collective-permute-start | bytes 491528 | tf_op jit(solution)/shard_map/ppermute | solution.py:359
  87.4 1.6 %collective-permute-done.1.refs_2_ = bf16[16,40,128]{2,1,0:T(8,128)(2,1)S(1)} collective-permute-done((bf16[16,40,128]{2,1,0:T(8,128)(2,1)S(1)}, bf16[16,40,128]{2,1,0:T(8,128)(2,1)S(1)}, u32[]{:S(2)}, u32[]{:S(2)}) %collective-permute-start.1) | collective-permute-done | bytes 163872 | tf_op jit(solution)/shard_map/ppermute | solution.py:362
  89.0 4.9 %collective-permute-start.2 = (bf16[16,40,128]{2,1,0:T(8,128)(2,1)S(1)}, bf16[16,40,128]{2,1,0:T(8,128)(2,1)S(1)}, u32[]{:S(2)}, u32[]{:S(2)}) collective-permute-start(bf16[16,40,128]{2,1,0:T(8,128)(2,1)S(1)} %collective-permute-done.1.refs_2_), channel_id=1, source_target_pairs={{0,56},{8,0},{16,8},{24,16},{32,24},{40,32},{48,40},{56,48},{1,57}... | collective-permute-start | bytes 491528 | tf_op jit(solution)/shard_map/ppermute | solution.py:362
  94.0 0.0 collective-permute-done.5.refs_5_
  94.0 1.9 %collective-permute-start.6 = (bf16[16,40,128]{2,1,0:T(8,128)(2,1)S(1)}, bf16[16,40,128]{2,1,0:T(8,128)(2,1)S(1)}, u32[]{:S(2)}, u32[]{:S(2)}) collective-permute-start(bf16[16,40,128]{2,1,0:T(8,128)(2,1)S(1)} %collective-permute-done.5.refs_5_), channel_id=1, source_target_pairs={{0,8},{8,16},{16,24},{24,32},{32,40},{40,48},{48,56},{56,0},{1,9},... | collective-permute-start | bytes 491528 | tf_op jit(solution)/shard_map/ppermute | solution.py:359
  95.9 0.9 collective-permute-done.2.refs_3_
  96.8 0.0 all-to-all-done.3.rows_ref
  96.8 5.6 %collective-permute-done.6.refs_4_ = bf16[16,40,128]{2,1,0:T(8,128)(2,1)S(1)} collective-permute-done((bf16[16,40,128]{2,1,0:T(8,128)(2,1)S(1)}, bf16[16,40,128]{2,1,0:T(8,128)(2,1)S(1)}, u32[]{:S(2)}, u32[]{:S(2)}) %collective-permute-start.6) | collective-permute-done | bytes 163872 | tf_op jit(solution)/shard_map/ppermute | solution.py:359
  102.4 0.0 copy-done
  102.4 0.0 copy-done.1
  102.4 0.0 copy-done.2
  102.4 0.0 copy-done.3
  102.4 0.0 copy-done.4
  102.4 0.0 copy-done.5
  102.5 0.0 copy-done.6
  102.5 0.0 copy-done.7
  102.5 2.4 %shard_map.199 = (f32[128,128]{1,0:T(8,128)}, f32[128,128]{1,0:T(8,128)}, f32[128,128]{1,0:T(8,128)}, f32[128,128]{1,0:T(8,128)}, bf16[2048,128]{1,0:T(8,128)(2,...) custom-call(s32[1]{0:T(128)} %bitcast.fs_ref, ...), custom_call_target="tpu_custom_call" | custom-call | flops 268435456 | bytes 1048576 | tf_op jit(solution)/shard_map/pallas_call | solution.py:154
Async XLA Ops:
  0.7 101.8 %copy-start = (bf16[2048,128]{1,0:T(8,128)(2,1)S(1)}, bf16[2048,128]{1,0:T(8,128)(2,1)}, u32[]{:S(2)}) copy-start(bf16[2048,128]{1,0:T(8,128)(2,1)} %basis_value_ref.3) | copy-start | bytes 1572868
  0.7 101.8 %copy-start.1 = (bf16[2048,128]{1,0:T(8,128)(2,1)S(1)}, bf16[2048,128]{1,0:T(8,128)(2,1)}, u32[]{:S(2)}) copy-start(bf16[2048,128]{1,0:T(8,128)(2,1)} %basis_output_ref.3) | copy-start | bytes 1572868
  0.7 101.7 %copy-start.2 = (f32[128,128]{1,0:T(8,128)S(1)}, f32[128,128]{1,0:T(8,128)}, u32[]{:S(2)}) copy-start(f32[128,128]{1,0:T(8,128)} %weight_value_ref.3) | copy-start | bytes 196612
  0.7 101.7 %copy-start.3 = (f32[128,128]{1,0:T(8,128)S(1)}, f32[128,128]{1,0:T(8,128)}, u32[]{:S(2)}) copy-start(f32[128,128]{1,0:T(8,128)} %weight_output_ref.3) | copy-start | bytes 196612
  0.7 101.7 %copy-start.4 = (f32[8,128]{1,0:T(8,128)S(1)}, f32[8,128]{1,0:T(8,128)}, u32[]{:S(2)}) copy-start(f32[8,128]{1,0:T(8,128)} %first_value_ref.3) | copy-start | bytes 12292
  0.7 101.7 %copy-start.5 = (f32[8,128]{1,0:T(8,128)S(1)}, f32[8,128]{1,0:T(8,128)}, u32[]{:S(2)}) copy-start(f32[8,128]{1,0:T(8,128)} %second_value_ref.3) | copy-start | bytes 12292
  0.7 101.7 %copy-start.6 = (f32[8,128]{1,0:T(8,128)S(1)}, f32[8,128]{1,0:T(8,128)}, u32[]{:S(2)}) copy-start(f32[8,128]{1,0:T(8,128)} %first_output_ref.3) | copy-start | bytes 12292
  0.7 101.7 %copy-start.7 = (f32[8,128]{1,0:T(8,128)S(1)}, f32[8,128]{1,0:T(8,128)}, u32[]{:S(2)}) copy-start(f32[8,128]{1,0:T(8,128)} %second_output_ref.3) | copy-start | bytes 12292
  48.4 14.8 %collective-permute-start.3 = (bf16[16,40,128]{2,1,0:T(8,128)(2,1)S(1)}, bf16[16,40,128]{2,1,0:T(8,128)(2,1)S(1)}, u32[]{:S(2)}, u32[]{:S(2)}) collective-permute-start(bf16[16,40,128]{2,1,0:T(8,128)(2,1)S(1)} %get-tuple-element.17.refs_0_), channel_id=1, source_target_pairs={{0,8},{8,16},{16,24},{24,32},{32,40},{40,48},{48,56},{56,0},{1,9},... | collective-permute-start | bytes 491528 | tf_op jit(solution)/shard_map/ppermute | solution.py:359
  51.9 14.5 %all-to-all-start.1 = ((f32[8,16,128]{2,1,0:T(8,128)}), f32[8,16,128]{2,1,0:T(8,128)S(1)}, u32[]{:S(2)}, u32[]{:S(2)}) async-start(f32[8,16,128]{2,1,0:T(8,128)} %get-tuple-element.14), calls=%async_computation.1 | async-start | bytes 131072 | tf_op jit(solution)/shard_map/all_to_all | solution.py:24
  58.1 23.4 %collective-permute-start = (bf16[16,40,128]{2,1,0:T(8,128)(2,1)S(1)}, bf16[16,40,128]{2,1,0:T(8,128)(2,1)S(1)}, u32[]{:S(2)}, u32[]{:S(2)}) collective-permute-start(bf16[16,40,128]{2,1,0:T(8,128)(2,1)S(1)} %get-tuple-element.17.refs_0_), channel_id=1, source_target_pairs={{0,56},{8,0},{16,8},{24,16},{32,24},{40,32},{48,40},{56,48},{1,57}... | collective-permute-start | bytes 491528 | tf_op jit(solution)/shard_map/ppermute | solution.py:362
  63.3 22.0 %collective-permute-start.4 = (bf16[16,40,128]{2,1,0:T(8,128)(2,1)S(1)}, bf16[16,40,128]{2,1,0:T(8,128)(2,1)S(1)}, u32[]{:S(2)}, u32[]{:S(2)}) collective-permute-start(bf16[16,40,128]{2,1,0:T(8,128)(2,1)S(1)} %collective-permute-done.3.refs_7_), channel_id=1, source_target_pairs={{0,8},{8,16},{16,24},{24,32},{32,40},{40,48},{48,56},{56,0},{1,9},... | collective-permute-start | bytes 491528 | tf_op jit(solution)/shard_map/ppermute | solution.py:359
  75.2 21.6 %all-to-all-start.3 = ((bf16[16,24,128]{2,1,0:T(8,128)(2,1)}), bf16[16,24,128]{2,1,0:T(8,128)(2,1)S(1)}, u32[]{:S(2)}, u32[]{:S(2)}) async-start(bf16[16,24,128]{2,1,0:T(8,128)(2,1)} %shard_map.198), calls=%async_computation.3 | async-start | bytes 196608 | tf_op jit(solution)/shard_map/all_to_all | solution.py:24
  81.5 7.5 %collective-permute-start.1 = (bf16[16,40,128]{2,1,0:T(8,128)(2,1)S(1)}, bf16[16,40,128]{2,1,0:T(8,128)(2,1)S(1)}, u32[]{:S(2)}, u32[]{:S(2)}) collective-permute-start(bf16[16,40,128]{2,1,0:T(8,128)(2,1)S(1)} %collective-permute-done.refs_1_), channel_id=1, source_target_pairs={{0,56},{8,0},{16,8},{24,16},{32,24},{40,32},{48,40},{56,48},{1,57}... | collective-permute-start | bytes 491528 | tf_op jit(solution)/shard_map/ppermute | solution.py:362
  85.3 8.7 %collective-permute-start.5 = (bf16[16,40,128]{2,1,0:T(8,128)(2,1)S(1)}, bf16[16,40,128]{2,1,0:T(8,128)(2,1)S(1)}, u32[]{:S(2)}, u32[]{:S(2)}) collective-permute-start(bf16[16,40,128]{2,1,0:T(8,128)(2,1)S(1)} %collective-permute-done.4.refs_6_), channel_id=1, source_target_pairs={{0,8},{8,16},{16,24},{24,32},{32,40},{40,48},{48,56},{56,0},{1,9},... | collective-permute-start | bytes 491528 | tf_op jit(solution)/shard_map/ppermute | solution.py:359
  89.0 7.8 %collective-permute-start.2 = (bf16[16,40,128]{2,1,0:T(8,128)(2,1)S(1)}, bf16[16,40,128]{2,1,0:T(8,128)(2,1)S(1)}, u32[]{:S(2)}, u32[]{:S(2)}) collective-permute-start(bf16[16,40,128]{2,1,0:T(8,128)(2,1)S(1)} %collective-permute-done.1.refs_2_), channel_id=1, source_target_pairs={{0,56},{8,0},{16,8},{24,16},{32,24},{40,32},{48,40},{56,48},{1,57}... | collective-permute-start | bytes 491528 | tf_op jit(solution)/shard_map/ppermute | solution.py:362
  94.0 8.4 %collective-permute-start.6 = (bf16[16,40,128]{2,1,0:T(8,128)(2,1)S(1)}, bf16[16,40,128]{2,1,0:T(8,128)(2,1)S(1)}, u32[]{:S(2)}, u32[]{:S(2)}) collective-permute-start(bf16[16,40,128]{2,1,0:T(8,128)(2,1)S(1)} %collective-permute-done.5.refs_5_), channel_id=1, source_target_pairs={{0,8},{8,16},{16,24},{24,32},{32,40},{40,48},{48,56},{56,0},{1,9},... | collective-permute-start | bytes 491528 | tf_op jit(solution)/shard_map/ppermute | solution.py:359

commit v5 on v4

--- a/solution.py
+++ b/solution.py
@@ -1,3 +1,5 @@
+import functools
+
 import jax
 import jax.numpy as jnp
 from jax import lax
@@ -163,83 +165,92 @@
     )(*inputs)
 
 
-def partial_kernel(
-    rep_ref,
-    hidden_ref,
-    grad_value_ref,
-    grad_output_ref,
-    mixed_ref,
-    basis_value_ref,
-    basis_output_ref,
-    weight_value_ref,
-    weight_output_ref,
-    first_value_ref,
-    second_value_ref,
-    first_output_ref,
-    second_output_ref,
-    out_ref,
-    hidden_sum_ref,
-    output_sum_ref,
-    old_ref,
-):
-    step = pl.program_id(0)
-    for tokens_ref, basis_ref, sum_ref in (
-        (hidden_ref, basis_value_ref, hidden_sum_ref),
-        (grad_output_ref, basis_output_ref, output_sum_ref),
-    ):
-        reduced = jnp.dot(tokens_ref[...], basis_ref[...], preferred_element_type=f32)
-
-        @pl.when(step == 0)
-        def _():
-            sum_ref[...] = reduced
-
-        @pl.when(step > 0)
-        def _():
-            sum_ref[...] += reduced
-
-    @pl.when(step == pl.num_programs(0) - 1)
-    def _():
-        products = []
-        for sum_ref, other_ref in (
-            (hidden_sum_ref, grad_value_ref),
-            (output_sum_ref, mixed_ref),
+def partial_kernel(rep_ref, *refs):
+    sources, (out_ref, *refs) = refs[:12], refs[12:]
+    tokens_refs, held_refs, refs = refs[:2], refs[2:12], refs[12:]
+    hidden_sum_ref, output_sum_ref, old_ref, first_sem, token_sem, later_sem = refs
+    basis_value_ref, basis_output_ref = held_refs[:2]
+    grad_value_ref, mixed_ref, weight_value_ref, weight_output_ref = held_refs[2:6]
+    olds = held_refs[6:]
+    steps, _, width = tokens_refs[0].shape
+
+    def token_copy(which, k):
+        columns = pl.ds(pl.multiple_of(k * width, width), width)
+        return pltpu.make_async_copy(
+            sources[which].at[:, columns], tokens_refs[which].at[k], token_sem.at[which, k]
+        )
+
+    first = [
+        pltpu.make_async_copy(sources[2 + n], held_refs[n], first_sem.at[n]) for n in range(2)
+    ]
+    later = [
+        pltpu.make_async_copy(sources[2 + n], held_refs[n], later_sem.at[n - 2])
+        for n in range(2, 10)
+    ]
+    for copy in first:
+        copy.start()
+    for k in range(steps):
+        for which in range(2):
+            token_copy(which, k).start()
+    for copy in later:
+        copy.start()
+    hidden_sum_ref[...] = jnp.zeros_like(hidden_sum_ref)
+    output_sum_ref[...] = jnp.zeros_like(output_sum_ref)
+    for copy in first:
+        copy.wait()
+
+    def multiply(k, carry):
+        here = pl.ds(pl.multiple_of(k * width, width), width)
+        for which, basis_ref, sum_ref in (
+            (0, basis_value_ref, hidden_sum_ref),
+            (1, basis_output_ref, output_sum_ref),
         ):
-            upper, lower = split(sum_ref[...])
-            other = other_ref[...]
-            products.append(
-                lax.dot_general(upper, other, contract_leading, preferred_element_type=f32)
-                + lax.dot_general(lower, other, contract_leading, preferred_element_type=f32)
+            token_copy(which, k).wait()
+            sum_ref[...] += jnp.dot(
+                tokens_refs[which][k], basis_ref[here, :], preferred_element_type=f32
             )
-        value, output = products
-        fs = out_ref.shape[0]
-        ranks, _ = first_value_ref.shape
-        count = 2 * ranks
-        rep, part, _ = old_ref.shape
-        cut = weight_value_ref.shape[0] // rep
-        run = min(part, ranks)
-        olds = (first_value_ref, second_value_ref, first_output_ref, second_output_ref)
-        for at in range(0, 4 * ranks, run):
-            from_row, to_row = at % ranks, at % part
-            old_ref[at // part, to_row : to_row + run, :] = olds[at // ranks][
-                from_row : from_row + run, :
-            ]
-        me = rep_ref[0]
-        piece = pl.ds(pl.multiple_of(me * cut, cut), cut)
-        piece_value = weight_value_ref[piece, :].astype(bf16)
-        piece_output = weight_output_ref[piece, :].astype(bf16)
-        old = old_ref[me]
-        upper = old.astype(bf16).astype(f32)
-        piece_old = jnp.concatenate([upper, old - upper]).astype(bf16)
-        weights_at = 2 * count
-        olds_at = weights_at + 2 * cut
-        for i in range(fs):
-            here = slice(i * ranks, (i + 1) * ranks)
-            upper, lower = split(jnp.concatenate([value[here], output[here]]))
-            out_ref[i, :count, :] = upper
-            out_ref[i, count:weights_at, :] = lower
-            out_ref[i, weights_at : weights_at + cut, :] = piece_value
-            out_ref[i, weights_at + cut : olds_at, :] = piece_output
-            out_ref[i, olds_at:, :] = piece_old
+        return carry
+
+    lax.fori_loop(0, steps, multiply, 0)
+    for copy in later:
+        copy.wait()
+    products = []
+    for sum_ref, other_ref in ((hidden_sum_ref, grad_value_ref), (output_sum_ref, mixed_ref)):
+        upper, lower = split(sum_ref[...])
+        other = other_ref[...]
+        products.append(
+            lax.dot_general(upper, other, contract_leading, preferred_element_type=f32)
+            + lax.dot_general(lower, other, contract_leading, preferred_element_type=f32)
+        )
+    value, output = products
+    fs = out_ref.shape[0]
+    ranks = olds[0].shape[0]
+    count = 2 * ranks
+    rep, part, _ = old_ref.shape
+    cut = weight_value_ref.shape[0] // rep
+    run = min(part, ranks)
+    for at in range(0, 4 * ranks, run):
+        from_row, to_row = at % ranks, at % part
+        old_ref[at // part, to_row : to_row + run, :] = olds[at // ranks][
+            from_row : from_row + run, :
+        ]
+    me = rep_ref[0]
+    piece = pl.ds(pl.multiple_of(me * cut, cut), cut)
+    piece_value = weight_value_ref[piece, :].astype(bf16)
+    piece_output = weight_output_ref[piece, :].astype(bf16)
+    old = old_ref[me]
+    upper = old.astype(bf16).astype(f32)
+    piece_old = jnp.concatenate([upper, old - upper]).astype(bf16)
+    weights_at = 2 * count
+    olds_at = weights_at + 2 * cut
+    for i in range(fs):
+        here = slice(i * ranks, (i + 1) * ranks)
+        upper, lower = split(jnp.concatenate([value[here], output[here]]))
+        out_ref[i, :count, :] = upper
+        out_ref[i, count:weights_at, :] = lower
+        out_ref[i, weights_at : weights_at + cut, :] = piece_value
+        out_ref[i, weights_at + cut : olds_at, :] = piece_output
+        out_ref[i, olds_at:, :] = piece_old
 
 
 def partial(rep_index, hidden, grad_value, grad_output, mixed, bases, weights, olds, fs, rep):
@@ -247,23 +258,21 @@
     rows, columns = weights[0].shape
     ranks = olds[0].shape[0]
     part = 4 * ranks // rep
-    steps = 4
-    block = depth // steps
-    wide = pl.BlockSpec((tokens, block), lambda i: (0, i))
-    basis = pl.BlockSpec((block, RANK), lambda i: (i, 0))
-    narrow = pl.BlockSpec((tokens, columns), lambda i: (0, 0))
-    weight = pl.BlockSpec((rows, columns), lambda i: (0, 0))
-    old = pl.BlockSpec((ranks, columns), lambda i: (0, 0))
+    steps = depth // 256
     height = 4 * ranks + 2 * (rows // rep) + 2 * part
+    held = (*bases, grad_value, mixed, *weights, *olds)
     return call(
         partial_kernel,
-        (rep_index, hidden, grad_value, grad_output, mixed, *bases, *weights, *olds),
+        (rep_index, hidden, grad_output, *held),
         [((fs, height, columns), bf16)],
-        specs=[smem, wide, narrow, wide, narrow, basis, basis, weight, weight] + [old] * 4,
-        scratch=[pltpu.VMEM((tokens, RANK), f32)] * 2 + [pltpu.VMEM((rep, part, columns), f32)],
+        specs=[smem] + [pl.BlockSpec(memory_space=pl.ANY)] * 12,
+        scratch=[pltpu.VMEM((steps, tokens, depth // steps), bf16)] * 2
+        + [pltpu.VMEM(a.shape, a.dtype) for a in held]
+        + [pltpu.VMEM((tokens, RANK), f32)] * 2
+        + [pltpu.VMEM((rep, part, columns), f32)]
+        + [pltpu.SemaphoreType.DMA(n) for n in ((2,), (2, steps), (8,))],
         flops=4 * tokens * depth * RANK,
         room=61,
-        grid=(steps,),
     )[0]
 
 
@@ -272,33 +281,34 @@
     total = mixed_ref[0, : 2 * count, :].astype(f32)
     for i in range(1, mixed_ref.shape[0]):
         total = total + mixed_ref[i, : 2 * count, :].astype(f32)
-    total = total[:count] + total[count:]
+    total = (total[:count] + total[count:]).astype(bf16)
     for j in range(out_ref.shape[0]):
         out_ref[j] = total
     pieces_ref[...] = mixed_ref[:, 2 * count :, :]
 
 
-def squares_kernel(sums_ref, whole_ref, squares_ref):
-    total = sums_ref[0]
-    for j in range(1, sums_ref.shape[0]):
-        total = total + sums_ref[j]
-    whole_ref[...] = total
-    squares = jnp.sum(total * total, keepdims=True)
-    squares_ref[...] = jnp.broadcast_to(squares[None], squares_ref.shape)
-
-
-def rows_kernel(whole_ref, squares_ref, out_ref):
-    count = whole_ref.shape[0]
-    total = squares_ref[0]
-    for t in range(1, squares_ref.shape[0]):
-        total = total + squares_ref[t]
-    total = total[:4]
-    upper = total.astype(bf16).astype(f32)
-    total = jnp.concatenate([upper, total - upper]).astype(bf16)
-    whole = whole_ref[...].astype(bf16)
+def rows_kernel(tp, tp_ref, sums_ref, whole_ref, out_ref):
+    members, count, columns = sums_ref.shape
+
+    def whole(t):
+        total = sums_ref[t].astype(f32)
+        for j in range(tp, members, tp):
+            total = total + sums_ref[j + t].astype(f32)
+        return total
+
+    squares = jnp.zeros((count, columns), f32)
+    for t in range(tp):
+        total = whole(t)
+        squares = squares + total * total
+    squares = jnp.broadcast_to(jnp.sum(squares, keepdims=True), (4, columns))
+    upper = squares.astype(bf16).astype(f32)
+    squares = jnp.concatenate([upper, squares - upper]).astype(bf16)
+    own = whole(tp_ref[0])
+    whole_ref[...] = own
+    own = own.astype(bf16)
     for i in range(out_ref.shape[0]):
-        out_ref[i, :count, :] = whole
-        out_ref[i, count:, :] = total
+        out_ref[i, :count, :] = own
+        out_ref[i, count:, :] = squares
 
 
 def local(
@@ -318,6 +328,7 @@
     fs, rep, tp = lax.axis_size("fs"), lax.axis_size("rep"), lax.axis_size("tp")
     fs_index = lax.axis_index("fs").astype(jnp.int32).reshape(1)
     rep_index = lax.axis_index("rep").astype(jnp.int32).reshape(1)
+    tp_index = lax.axis_index("tp").astype(jnp.int32).reshape(1)
     rows, columns = weight_value.shape
     ranks = first_value.shape[0]
 
@@ -343,14 +354,15 @@
     summed, piece = call(
         sum_kernel,
         (mixed,),
-        [((rep, count, columns), f32), ((fs, height, columns), bf16)],
-    )
-    summed = exchange(summed, "rep")
-    whole, squares = call(
-        squares_kernel, (summed,), [((count, columns), f32), ((tp, 8, columns), f32)]
-    )
-    squares = exchange(squares, "tp")
-    rowed = call(rows_kernel, (whole, squares), [((fs, count + 8, columns), bf16)])[0]
+        [((rep * tp, count, columns), bf16), ((fs, height, columns), bf16)],
+    )
+    summed = exchange(summed, ("rep", "tp"))
+    whole, rowed = call(
+        functools.partial(rows_kernel, tp),
+        (tp_index, summed),
+        [((count, columns), f32), ((fs, count + 8, columns), bf16)],
+        specs=[smem, vmem],
+    )
     gathered = exchange(rowed, "fs")
 
     pieces = [piece] + [None] * (rep - 1)

time: 106 us -> 108 us (1.019)
  blocking collectives: 46.2 us -> 38.3 us
  starting transfers between devices: 35.8 us -> 40.3 us
  waiting for transfers between devices: 9.35 us -> 13.2 us
  Pallas kernels: 12.6 us -> 15.1 us
    all_to_all x2 -> x1, blocking collectives: 46.2 us -> 38.3 us  [exchange(): return lax.all_to_all(chunks, axes, 0, 0, tiled=True)]
    ppermute x4, waiting for transfers between devices: 5.62 us -> 11.5 us  [local(): up = lax.ppermute(up, 'rep', [(r, (r + 1) % rep) for r in range(rep)])]
    all_to_all x2, starting transfers between devices: 12.5 us -> 16.8 us  [exchange(): return lax.all_to_all(chunks, axes, 0, 0, tiled=True)]
    pallas_call x5 -> x4, Pallas kernels: 12.6 us -> 15.1 us  [call(): pl.pallas_call(kernel, out_shape=outs, in_specs=[vmem] * len(inputs) if s...]
    all_to_all x2, waiting for transfers between devices: 1.23 us -> 0.01 us  [exchange(): return lax.all_to_all(chunks, axes, 0, 0, tiled=True)]
where the time goes in v5:
time: 108 us
  starting transfers between devices  40.3 us (37%)
  blocking collectives  38.3 us (35%)
  Pallas kernels  15.1 us (14%)
  waiting for transfers between devices  13.2 us (12%)
    all_to_all x1, blocking collectives, exchange(): return lax.all_to_all(chunks, axes, 0, 0, tiled=True)  38.3 us
    all_to_all x2, starting transfers between devices, exchange(): return lax.all_to_all(chunks, axes, 0, 0, tiled=True)  16.8 us
    pallas_call x4, Pallas kernels, call(): pl.pallas_call(kernel, out_shape=outs, in_specs=[vmem] * len(inputs) if s...  15.1 us
    ppermute x3, starting transfers between devices, local(): down = lax.ppermute(down, 'rep', [(r, (r - 1) % rep) for r in range(rep)])  14.4 us
    ppermute x4, waiting for transfers between devices, local(): up = lax.ppermute(up, 'rep', [(r, (r + 1) % rep) for r in range(rep)])  11.5 us
    ppermute x4, starting transfers between devices, local(): up = lax.ppermute(up, 'rep', [(r, (r + 1) % rep) for r in range(rep)])  9.11 us
  transfers between devices with their start and end apart: 9, of which 4 were waited for; matrix products, arithmetic and copies ran while one was open for 0% of the time, Pallas kernels for 1%

profile of v5, /device:TPU:6, one launch (start us, length us, event | category | flops | bytes accessed | tf_op | source)
XLA Modules:
  0.0 107.8 jit_solution(3732921999131312987)
XLA Ops:
  0.7 0.0 copy-start
  0.7 0.0 copy-start.1
  0.7 0.0 copy-start.2
  0.7 0.0 copy-start.3
  0.7 0.0 copy-start.4
  0.7 0.0 copy-start.5
  0.7 0.0 copy-start.6
  0.7 0.0 copy-start.7
  0.7 11.2 %shard_map.195 = bf16[16,72,128]{2,1,0:T(8,128)(2,1)} custom-call(s32[1]{0:T(128)} %bitcast.1.rep_ref, bf16[896,2048]{1,0:T(8,128)(2,1)} %refs_0_.1, bf16[896,2048]{1,0:T(8,128)(2,1)} %refs_1_.1, bf16[2048,128]{1,0:T(8,128)(2,1)} %basis_value_ref.1, bf16[2048,128]{1,0:T(8,128)(2,1)} %basis_output_ref.1, bf16[896,128]{1,0:T(8,128)(2,1)} %refs_4_.1, ...), custom_call_target="tpu_custom_call" | custom-call | flops 939524096 | bytes 1048576 | tf_op jit(solution)/shard_map/pallas_call | solution.py:156
  11.9 38.3 %all_to_all.15.mixed_ref = bf16[16,72,128]{2,1,0:T(8,128)(2,1)S(1)} all-to-all(bf16[16,72,128]{2,1,0:T(8,128)(2,1)} %shard_map.195), channel_id=1, replica_groups=mesh['fs'=16,'rep'=8,'tp'=8] {'fs'}, dimensions={0} | all-to-all | bytes 589824 | tf_op jit(solution)/shard_map/all_to_all | solution.py:26
  50.2 0.7 shard_map.196
  51.0 10.6 %all-to-all-start.1 = ((bf16[64,16,128]{2,1,0:T(8,128)(2,1)}), bf16[64,16,128]{2,1,0:T(8,128)(2,1)S(1)}, u32[]{:S(2)}, u32[]{:S(2)}) async-start(bf16[64,16,128]{2,1,0:T(8,128)(2,1)} %get-tuple-element.14), calls=%async_computation.1 | async-start | bytes 524288 | tf_op jit(solution)/shard_map/all_to_all | solution.py:26
  61.6 3.4 %collective-permute-start.3 = (bf16[16,40,128]{2,1,0:T(8,128)(2,1)S(1)}, bf16[16,40,128]{2,1,0:T(8,128)(2,1)S(1)}, u32[]{:S(2)}, u32[]{:S(2)}) collective-permute-start(bf16[16,40,128]{2,1,0:T(8,128)(2,1)S(1)} %get-tuple-element.17.refs_0_), channel_id=1, source_target_pairs={{0,8},{8,16},{16,24},{24,32},{32,40},{40,48},{48,56},{56,0},{1,9},... | collective-permute-start | bytes 491528 | tf_op jit(solution)/shard_map/ppermute | solution.py:371
  64.9 3.7 %collective-permute-start = (bf16[16,40,128]{2,1,0:T(8,128)(2,1)S(1)}, bf16[16,40,128]{2,1,0:T(8,128)(2,1)S(1)}, u32[]{:S(2)}, u32[]{:S(2)}) collective-permute-start(bf16[16,40,128]{2,1,0:T(8,128)(2,1)S(1)} %get-tuple-element.17.refs_0_), channel_id=1, source_target_pairs={{0,56},{8,0},{16,8},{24,16},{32,24},{40,32},{48,40},{56,48},{1,57}... | collective-permute-start | bytes 491528 | tf_op jit(solution)/shard_map/ppermute | solution.py:374
  68.6 5.8 %collective-permute-done.3.refs_7_ = bf16[16,40,128]{2,1,0:T(8,128)(2,1)S(1)} collective-permute-done((bf16[16,40,128]{2,1,0:T(8,128)(2,1)S(1)}, bf16[16,40,128]{2,1,0:T(8,128)(2,1)S(1)}, u32[]{:S(2)}, u32[]{:S(2)}) %collective-permute-start.3) | collective-permute-done | bytes 163872 | tf_op jit(solution)/shard_map/ppermute | solution.py:371
  74.5 1.9 %collective-permute-start.4 = (bf16[16,40,128]{2,1,0:T(8,128)(2,1)S(1)}, bf16[16,40,128]{2,1,0:T(8,128)(2,1)S(1)}, u32[]{:S(2)}, u32[]{:S(2)}) collective-permute-start(bf16[16,40,128]{2,1,0:T(8,128)(2,1)S(1)} %collective-permute-done.3.refs_7_), channel_id=1, source_target_pairs={{0,8},{8,16},{16,24},{24,32},{32,40},{40,48},{48,56},{56,0},{1,9},... | collective-permute-start | bytes 491528 | tf_op jit(solution)/shard_map/ppermute | solution.py:371
  76.4 0.0 all-to-all-done.1.sums_ref
  76.4 0.8 shard_map.197
  77.2 6.2 %all-to-all-start.2 = ((bf16[16,24,128]{2,1,0:T(8,128)(2,1)}), bf16[16,24,128]{2,1,0:T(8,128)(2,1)S(1)}, u32[]{:S(2)}, u32[]{:S(2)}) async-start(bf16[16,24,128]{2,1,0:T(8,128)(2,1)} %get-tuple-element.15), calls=%async_computation.2 | async-start | bytes 196608 | tf_op jit(solution)/shard_map/all_to_all | solution.py:26
  83.4 0.0 collective-permute-done.refs_1_
  83.4 5.1 %collective-permute-start.1 = (bf16[16,40,128]{2,1,0:T(8,128)(2,1)S(1)}, bf16[16,40,128]{2,1,0:T(8,128)(2,1)S(1)}, u32[]{:S(2)}, u32[]{:S(2)}) collective-permute-start(bf16[16,40,128]{2,1,0:T(8,128)(2,1)S(1)} %collective-permute-done.refs_1_), channel_id=1, source_target_pairs={{0,56},{8,0},{16,8},{24,16},{32,24},{40,32},{48,40},{56,48},{1,57}... | collective-permute-start | bytes 491528 | tf_op jit(solution)/shard_map/ppermute | solution.py:374
  88.5 0.0 collective-permute-done.4.refs_6_
  88.5 1.9 %collective-permute-start.5 = (bf16[16,40,128]{2,1,0:T(8,128)(2,1)S(1)}, bf16[16,40,128]{2,1,0:T(8,128)(2,1)S(1)}, u32[]{:S(2)}, u32[]{:S(2)}) collective-permute-start(bf16[16,40,128]{2,1,0:T(8,128)(2,1)S(1)} %collective-permute-done.4.refs_6_), channel_id=1, source_target_pairs={{0,8},{8,16},{16,24},{24,32},{32,40},{40,48},{48,56},{56,0},{1,9},... | collective-permute-start | bytes 491528 | tf_op jit(solution)/shard_map/ppermute | solution.py:371
  90.5 0.9 collective-permute-done.1.refs_2_
  91.4 5.6 %collective-permute-start.2 = (bf16[16,40,128]{2,1,0:T(8,128)(2,1)S(1)}, bf16[16,40,128]{2,1,0:T(8,128)(2,1)S(1)}, u32[]{:S(2)}, u32[]{:S(2)}) collective-permute-start(bf16[16,40,128]{2,1,0:T(8,128)(2,1)S(1)} %collective-permute-done.1.refs_2_), channel_id=1, source_target_pairs={{0,56},{8,0},{16,8},{24,16},{32,24},{40,32},{48,40},{56,48},{1,57}... | collective-permute-start | bytes 491528 | tf_op jit(solution)/shard_map/ppermute | solution.py:374
  96.9 0.0 collective-permute-done.5.refs_5_
  97.0 1.9 %collective-permute-start.6 = (bf16[16,40,128]{2,1,0:T(8,128)(2,1)S(1)}, bf16[16,40,128]{2,1,0:T(8,128)(2,1)S(1)}, u32[]{:S(2)}, u32[]{:S(2)}) collective-permute-start(bf16[16,40,128]{2,1,0:T(8,128)(2,1)S(1)} %collective-permute-done.5.refs_5_), channel_id=1, source_target_pairs={{0,8},{8,16},{16,24},{24,32},{32,40},{40,48},{48,56},{56,0},{1,9},... | collective-permute-start | bytes 491528 | tf_op jit(solution)/shard_map/ppermute | solution.py:371
  98.9 0.9 collective-permute-done.2.refs_3_
  99.8 5.6 %collective-permute-done.6.refs_4_ = bf16[16,40,128]{2,1,0:T(8,128)(2,1)S(1)} collective-permute-done((bf16[16,40,128]{2,1,0:T(8,128)(2,1)S(1)}, bf16[16,40,128]{2,1,0:T(8,128)(2,1)S(1)}, u32[]{:S(2)}, u32[]{:S(2)}) %collective-permute-start.6) | collective-permute-done | bytes 163872 | tf_op jit(solution)/shard_map/ppermute | solution.py:371
  105.4 0.0 all-to-all-done.2.rows_ref
  105.4 0.0 copy-done
  105.4 0.0 copy-done.1
  105.4 0.0 copy-done.2
  105.4 0.0 copy-done.3
  105.4 0.0 copy-done.4
  105.4 0.0 copy-done.5
  105.4 0.0 copy-done.6
  105.4 0.0 copy-done.7
  105.5 2.4 %shard_map.198 = (f32[128,128]{1,0:T(8,128)}, f32[128,128]{1,0:T(8,128)}, f32[128,128]{1,0:T(8,128)}, f32[128,128]{1,0:T(8,128)}, bf16[2048,128]{1,0:T(8,128)(2,...) custom-call(s32[1]{0:T(128)} %bitcast.fs_ref, ...), custom_call_target="tpu_custom_call" | custom-call | flops 268435456 | bytes 1048576 | tf_op jit(solution)/shard_map/pallas_call | solution.py:156
Async XLA Ops:
  0.7 104.7 %copy-start = (bf16[2048,128]{1,0:T(8,128)(2,1)S(1)}, bf16[2048,128]{1,0:T(8,128)(2,1)}, u32[]{:S(2)}) copy-start(bf16[2048,128]{1,0:T(8,128)(2,1)} %basis_value_ref.1) | copy-start | bytes 1572868
  0.7 104.7 %copy-start.1 = (bf16[2048,128]{1,0:T(8,128)(2,1)S(1)}, bf16[2048,128]{1,0:T(8,128)(2,1)}, u32[]{:S(2)}) copy-start(bf16[2048,128]{1,0:T(8,128)(2,1)} %basis_output_ref.1) | copy-start | bytes 1572868
  0.7 104.7 %copy-start.2 = (f32[128,128]{1,0:T(8,128)S(1)}, f32[128,128]{1,0:T(8,128)}, u32[]{:S(2)}) copy-start(f32[128,128]{1,0:T(8,128)} %weight_value_ref.1) | copy-start | bytes 196612
  0.7 104.7 %copy-start.3 = (f32[128,128]{1,0:T(8,128)S(1)}, f32[128,128]{1,0:T(8,128)}, u32[]{:S(2)}) copy-start(f32[128,128]{1,0:T(8,128)} %weight_output_ref.1) | copy-start | bytes 196612
  0.7 104.7 %copy-start.4 = (f32[8,128]{1,0:T(8,128)S(1)}, f32[8,128]{1,0:T(8,128)}, u32[]{:S(2)}) copy-start(f32[8,128]{1,0:T(8,128)} %first_value_ref.1) | copy-start | bytes 12292
  0.7 104.7 %copy-start.5 = (f32[8,128]{1,0:T(8,128)S(1)}, f32[8,128]{1,0:T(8,128)}, u32[]{:S(2)}) copy-start(f32[8,128]{1,0:T(8,128)} %second_value_ref.1) | copy-start | bytes 12292
  0.7 104.7 %copy-start.6 = (f32[8,128]{1,0:T(8,128)S(1)}, f32[8,128]{1,0:T(8,128)}, u32[]{:S(2)}) copy-start(f32[8,128]{1,0:T(8,128)} %first_output_ref.1) | copy-start | bytes 12292
  0.7 104.7 %copy-start.7 = (f32[8,128]{1,0:T(8,128)S(1)}, f32[8,128]{1,0:T(8,128)}, u32[]{:S(2)}) copy-start(f32[8,128]{1,0:T(8,128)} %second_output_ref.1) | copy-start | bytes 12292
  51.0 25.4 %all-to-all-start.1 = ((bf16[64,16,128]{2,1,0:T(8,128)(2,1)}), bf16[64,16,128]{2,1,0:T(8,128)(2,1)S(1)}, u32[]{:S(2)}, u32[]{:S(2)}) async-start(bf16[64,16,128]{2,1,0:T(8,128)(2,1)} %get-tuple-element.14), calls=%async_computation.1 | async-start | bytes 524288 | tf_op jit(solution)/shard_map/all_to_all | solution.py:26
  61.6 12.9 %collective-permute-start.3 = (bf16[16,40,128]{2,1,0:T(8,128)(2,1)S(1)}, bf16[16,40,128]{2,1,0:T(8,128)(2,1)S(1)}, u32[]{:S(2)}, u32[]{:S(2)}) collective-permute-start(bf16[16,40,128]{2,1,0:T(8,128)(2,1)S(1)} %get-tuple-element.17.refs_0_), channel_id=1, source_target_pairs={{0,8},{8,16},{16,24},{24,32},{32,40},{40,48},{48,56},{56,0},{1,9},... | collective-permute-start | bytes 491528 | tf_op jit(solution)/shard_map/ppermute | solution.py:371
  64.9 18.4 %collective-permute-start = (bf16[16,40,128]{2,1,0:T(8,128)(2,1)S(1)}, bf16[16,40,128]{2,1,0:T(8,128)(2,1)S(1)}, u32[]{:S(2)}, u32[]{:S(2)}) collective-permute-start(bf16[16,40,128]{2,1,0:T(8,128)(2,1)S(1)} %get-tuple-element.17.refs_0_), channel_id=1, source_target_pairs={{0,56},{8,0},{16,8},{24,16},{32,24},{40,32},{48,40},{56,48},{1,57}... | collective-permute-start | bytes 491528 | tf_op jit(solution)/shard_map/ppermute | solution.py:374
  74.5 14.1 %collective-permute-start.4 = (bf16[16,40,128]{2,1,0:T(8,128)(2,1)S(1)}, bf16[16,40,128]{2,1,0:T(8,128)(2,1)S(1)}, u32[]{:S(2)}, u32[]{:S(2)}) collective-permute-start(bf16[16,40,128]{2,1,0:T(8,128)(2,1)S(1)} %collective-permute-done.3.refs_7_), channel_id=1, source_target_pairs={{0,8},{8,16},{16,24},{24,32},{32,40},{40,48},{48,56},{56,0},{1,9},... | collective-permute-start | bytes 491528 | tf_op jit(solution)/shard_map/ppermute | solution.py:371
  77.2 28.2 %all-to-all-start.2 = ((bf16[16,24,128]{2,1,0:T(8,128)(2,1)}), bf16[16,24,128]{2,1,0:T(8,128)(2,1)S(1)}, u32[]{:S(2)}, u32[]{:S(2)}) async-start(bf16[16,24,128]{2,1,0:T(8,128)(2,1)} %get-tuple-element.15), calls=%async_computation.2 | async-start | bytes 196608 | tf_op jit(solution)/shard_map/all_to_all | solution.py:26
  83.4 8.0 %collective-permute-start.1 = (bf16[16,40,128]{2,1,0:T(8,128)(2,1)S(1)}, bf16[16,40,128]{2,1,0:T(8,128)(2,1)S(1)}, u32[]{:S(2)}, u32[]{:S(2)}) collective-permute-start(bf16[16,40,128]{2,1,0:T(8,128)(2,1)S(1)} %collective-permute-done.refs_1_), channel_id=1, source_target_pairs={{0,56},{8,0},{16,8},{24,16},{32,24},{40,32},{48,40},{56,48},{1,57}... | collective-permute-start | bytes 491528 | tf_op jit(solution)/shard_map/ppermute | solution.py:374
  88.5 8.4 %collective-permute-start.5 = (bf16[16,40,128]{2,1,0:T(8,128)(2,1)S(1)}, bf16[16,40,128]{2,1,0:T(8,128)(2,1)S(1)}, u32[]{:S(2)}, u32[]{:S(2)}) collective-permute-start(bf16[16,40,128]{2,1,0:T(8,128)(2,1)S(1)} %collective-permute-done.4.refs_6_), channel_id=1, source_target_pairs={{0,8},{8,16},{16,24},{24,32},{32,40},{40,48},{48,56},{56,0},{1,9},... | collective-permute-start | bytes 491528 | tf_op jit(solution)/shard_map/ppermute | solution.py:371
  91.4 8.4 %collective-permute-start.2 = (bf16[16,40,128]{2,1,0:T(8,128)(2,1)S(1)}, bf16[16,40,128]{2,1,0:T(8,128)(2,1)S(1)}, u32[]{:S(2)}, u32[]{:S(2)}) collective-permute-start(bf16[16,40,128]{2,1,0:T(8,128)(2,1)S(1)} %collective-permute-done.1.refs_2_), channel_id=1, source_target_pairs={{0,56},{8,0},{16,8},{24,16},{32,24},{40,32},{48,40},{56,48},{1,57}... | collective-permute-start | bytes 491528 | tf_op jit(solution)/shard_map/ppermute | solution.py:374
  97.0 8.4 %collective-permute-start.6 = (bf16[16,40,128]{2,1,0:T(8,128)(2,1)S(1)}, bf16[16,40,128]{2,1,0:T(8,128)(2,1)S(1)}, u32[]{:S(2)}, u32[]{:S(2)}) collective-permute-start(bf16[16,40,128]{2,1,0:T(8,128)(2,1)S(1)} %collective-permute-done.5.refs_5_), channel_id=1, source_target_pairs={{0,8},{8,16},{16,24},{24,32},{32,40},{40,48},{48,56},{56,0},{1,9},... | collective-permute-start | bytes 491528 | tf_op jit(solution)/shard_map/ppermute | solution.py:371
